TPU v7x, 32 devices: a whole 2x2x4 slice. The times are simulated.
32 devices in a mesh: sp: 16 (over z, y, x), tp: 2 (over core).
Axes of the slice: x: 2, y: 2, z: 4, core: 2. Of those that a mesh axis runs over, the one named last changes fastest.
Arguments:
- prompt: bfloat16 [8, 1024, 2048], P(None, 'sp'), may hold values from -6 to 6
- keep_scale: float32 [8, 1024], P(None, 'sp'), may hold values from 0.25 to 1
- new_token: bfloat16 [8, 2048], P(None, 'tp'), may hold values from -6 to 6
- w_query: bfloat16 [2048, 1024], P(None, 'tp'), may hold values from -0.125 to 0.125
- w_forget: bfloat16 [2048, 1024], P(None, 'tp'), may hold values from -0.125 to 0.125
- w_value: bfloat16 [2048, 1024], P(None, 'tp'), may hold values from -2.109375 to 2.109375
- w_outgate: bfloat16 [2048, 1024], P(None, 'tp'), may hold values from -0.125 to 0.125
- floor_gap: float32 [1024], P('tp'), may hold values from 0 to 0.06
- norm_gain: float32 [128], replicated, may hold values from 0.1 to 1.9
Outputs:
- state_cache: bfloat16 [8, 1024, 128], P('tp', 'sp')
- first_read: bfloat16 [8, 1024], P(None, 'tp')
All inputs are finite; a program needn't handle non-finite values.
Results may differ from a plain program's by a relative error of at most 0.0022.
The roundings to bfloat16 on the way count: a program that leaves them out, or rounds other values in their place, can miss the bound.
Values may be sent and summed in bfloat16 or wider, within the bound.
A program may use at most 64 MiB of HBM per device.

v0:
```python
import functools

import jax
import jax.numpy as jnp
from jax import lax
from jax.experimental import pallas as pl
from jax.experimental.pallas import tpu as pltpu
from jax.sharding import PartitionSpec as P

EPSILON = 1e-06
MESH = pl.DeviceIdType.MESH
F32 = jnp.float32
BF16 = jnp.bfloat16


def partner(mine, step, count):
    total, bit = 0, 1
    while bit < count:
        total = total + bit * lax.rem(lax.rem(mine // bit, 2) + lax.rem(step // bit, 2), 2)
        bit *= 2
    return total


def pieces(x, count):
    out = []
    for _ in range(count):
        piece = x.astype(BF16)
        out.append(piece)
        x = x - piece.astype(F32)
    return out


def kernel(
    sizes,
    prompt, keep, token, w_query, w_forget, w_value, w_outgate, floor, gain,
    cache_out, read_out,
    blocks, keeps, tokens, wq, wf, wv, wo, weighted, values, logs, totals, got_totals, states, got_states, reads, sums,
    local_sem, direct_send, direct_recv, keep_send, keep_recv, fwd_send, fwd_recv,
    token_send, token_recv, total_send, total_recv, row_send, row_recv, state_send, state_recv, read_send, read_recv,
):
    n, t, s_count, members, group, heads, head, rows = sizes
    planes = n // members
    me, core = lax.axis_index("sp"), lax.axis_index("tp")
    plane, place = me // members, lax.rem(me, members)
    model = prompt.shape[2]
    part = model // t
    positions = prompt.shape[1]
    width = heads * head
    side = 2
    batches = 2 if heads % 2 == 0 else 1
    batch = heads // batches

    def class_of(p):
        return lax.rem(p, side) * (members // side) + p // side

    def member_of(q):
        return (q % (members // side)) * side + q // (members // side)

    def turn(a, z):
        return (1 + a + (2 * z) // planes) % 2

    def prompt_of(p, a):
        return class_of(p) + members * turn(a, plane)

    def columns(c):
        return pl.ds(pl.multiple_of(c * part, part), part)

    def peer(r):
        return partner(place, r, members)

    local = [
        pltpu.make_async_copy(prompt.at[prompt_of(place, 0)], blocks.at[0, place], local_sem.at[0]),
        pltpu.make_async_copy(prompt.at[prompt_of(place, 1)], blocks.at[1, place], local_sem.at[1]),
        pltpu.make_async_copy(w_forget, wf, local_sem.at[2]),
        pltpu.make_async_copy(w_value, wv, local_sem.at[3]),
        pltpu.make_async_copy(w_query, wq, local_sem.at[4]),
        pltpu.make_async_copy(w_outgate, wo, local_sem.at[5]),
    ]

    barrier = pltpu.get_barrier_semaphore()
    for o in range(1, n):
        pl.semaphore_signal(barrier, inc=1, device_id=(lax.rem(me + o, n), core), device_id_type=MESH)
    for o in range(1, t):
        pl.semaphore_signal(barrier, inc=1, device_id=(me, lax.rem(core + o, t)), device_id_type=MESH)
    for copy in local:
        copy.start()
    pl.semaphore_wait(barrier, n - 1 + t - 1)

    def direct(a, r):
        to = peer(r)
        return pltpu.make_async_remote_copy(
            src_ref=prompt.at[prompt_of(to, a), :, columns(core)],
            dst_ref=blocks.at[a, place, :, columns(core)],
            send_sem=direct_send.at[a, r], recv_sem=direct_recv.at[a, r],
            device_id=(plane * members + to, core), device_id_type=MESH,
        )

    def direct_in(a, r):
        frm = peer(r)
        return pltpu.make_async_remote_copy(
            src_ref=prompt.at[prompt_of(frm, a), :, columns(core)],
            dst_ref=blocks.at[a, frm, :, columns(core)],
            send_sem=direct_send.at[a, r], recv_sem=direct_recv.at[a, r],
            device_id=(plane * members + frm, core), device_id_type=MESH,
        )

    def keep_copy(r):
        return pltpu.make_async_remote_copy(
            src_ref=keep, dst_ref=keeps.at[r],
            send_sem=keep_send.at[r], recv_sem=keep_recv.at[r],
            device_id=(plane * members + peer(r), core), device_id_type=MESH,
        )

    def forward(a, r, o, c):
        piece = blocks.at[a, peer(r), :, columns(c)]
        return pltpu.make_async_remote_copy(
            src_ref=piece, dst_ref=piece,
            send_sem=fwd_send.at[a, r, o], recv_sem=fwd_recv.at[a, r, o],
            device_id=(me, lax.rem(core + o, t)), device_id_type=MESH,
        )

    def token_copy(o, c):
        return pltpu.make_async_remote_copy(
            src_ref=token, dst_ref=tokens.at[c],
            send_sem=token_send.at[o], recv_sem=token_recv.at[o],
            device_id=(me, lax.rem(core + o, t)), device_id_type=MESH,
        )

    for r in range(1, members):
        keep_copy(r).start()
    for a in range(2):
        for r in range(1, members):
            direct(a, r).start()
    for o in range(1, t):
        token_copy(o, core).start()

    keeps[0] = keep[...]
    tokens[core] = token[...]
    floor_row = floor[...]

    def value(a, r):
        p = peer(r)
        values[a, p] = jnp.dot(blocks[a, p], wv[...], preferred_element_type=F32).astype(BF16)

    def forget(a, r):
        p = peer(r)
        pre = jnp.dot(blocks[a, p], wf[...], preferred_element_type=F32)
        loss = floor_row * (1.0 / (1.0 + jnp.exp(pre)))
        row = keeps[r, pl.ds(prompt_of(place, a), 1), :]
        i0 = lax.broadcasted_iota(jnp.int32, (positions, positions), 0)
        i1 = lax.broadcasted_iota(jnp.int32, (positions, positions), 1)
        scale = jnp.sum(jnp.where(i0 == i1, jnp.broadcast_to(row, (positions, positions)), 0.0), axis=1, keepdims=True)
        log_forget = jnp.log(scale) + jnp.log1p(-loss)
        gate = 1.0 - scale + scale * loss
        later = jnp.where(i1 > i0, 1.0, 0.0).astype(BF16)
        inside = sum(jnp.dot(later, piece, preferred_element_type=F32) for piece in pieces(log_forget, 3))
        logs[a, pl.ds(p, 1), :] = inside[0:1] + log_forget[0:1]
        weighted[a, p] = gate * jnp.exp(inside)

    def total_copy(k, o, z):
        return pltpu.make_async_remote_copy(
            src_ref=totals.at[k, z], dst_ref=totals.at[k, z],
            send_sem=total_send.at[k, o], recv_sem=total_recv.at[k, o],
            device_id=(lax.rem(me + o * members, n), core), device_id_type=MESH,
        )

    def keeper(a, g):
        return prompt_of(place, a) * group + g

    def row_copy(a, g):
        return pltpu.make_async_remote_copy(
            src_ref=totals.at[turn(a, plane), plane], dst_ref=got_totals.at[plane],
            send_sem=row_send.at[a, g], recv_sem=row_recv.at[plane],
            device_id=(keeper(a, g), core), device_id_type=MESH,
        )

    def state_copy(a, g, b):
        return pltpu.make_async_remote_copy(
            src_ref=states.at[a, pl.ds(b * batch, batch), pl.ds(g * rows, rows), :],
            dst_ref=got_states.at[plane, pl.ds(b * batch, batch)],
            send_sem=state_send.at[a, g, b], recv_sem=state_recv.at[plane, b],
            device_id=(keeper(a, g), core), device_id_type=MESH,
        )

    def read_copy(o, sender):
        return pltpu.make_async_remote_copy(
            src_ref=reads.at[sender], dst_ref=reads.at[sender],
            send_sem=read_send.at[o], recv_sem=read_recv.at[o],
            device_id=(lax.rem(me + o, n), core), device_id_type=MESH,
        )

    def finish(a):
        suffixes, suffix = [None] * members, jnp.zeros((1, width), F32)
        for p in reversed(range(members)):
            suffixes[p] = suffix
            suffix = suffix + logs[a, p : p + 1, :]
        k = turn(a, plane)
        totals[k, plane] = suffix
        for o in range(1, planes):
            total_copy(k, o, plane).start()
        value(a, members - 1)
        for p in range(members):
            weighted[a, p] = weighted[a, p] * jnp.exp(suffixes[p])
        for h in range(heads):
            lanes = slice(h * head, (h + 1) * head)
            w = weighted[a, :, :, lanes].reshape(members * positions, head)
            v = values[a, :, :, lanes].reshape(members * positions, head)
            states[a, h] = sum(
                lax.dot_general(piece, v, (((0,), (0,)), ((), ())), preferred_element_type=F32)
                for piece in pieces(w, 2)
            )
        for g in range(group):

            @pl.when(keeper(a, g) != me)
            def _():
                row_copy(a, g).start()
                for b in range(batches if a == 0 else 1):
                    state_copy(a, g, b).start()

            @pl.when(keeper(a, g) == me)
            def _():
                got_totals[plane] = suffix
                got_states[plane] = states[a, :, g * rows : (g + 1) * rows, :]

    def send_reads():
        for o in range(1, planes):
            z = lax.rem(plane - o + planes, planes)
            for k in range(2):
                total_copy(k, o, z).wait_recv()
        for a in range(2):
            later = jnp.zeros((1, width), F32)
            for z in range(planes):
                later = later + jnp.where(z > plane, totals[turn(a, plane), z], 0.0)
            decay = jnp.exp(later)
            for h in range(heads):
                lanes = slice(h * head, (h + 1) * head)
                reads[me, a, :, lanes] = jnp.dot(
                    sums[3 + a, :, lanes] * decay[:, lanes], states[a, h],
                    preferred_element_type=F32, precision=lax.Precision.HIGHEST,
                )[0:1]
        for o in range(n - 1, 0, -1):
            read_copy(o, me).start()
        for g in range(group):

            @pl.when(keeper(1, g) != me)
            def _():
                for b in range(1, batches):
                    state_copy(1, g, b).start()

    for copy in local[:4]:
        copy.wait()

    def own_block(a, carry):
        forget(a, 0)
        value(a, 0)
        return carry

    lax.fori_loop(0, 2, own_block, 0)

    local[4].wait()
    local[5].wait()
    for o in range(1, t):
        token_copy(o, lax.rem(core - o + t, t)).wait_recv()
    feature = jnp.concatenate([tokens[c] for c in range(t)], axis=1)
    query = jnp.dot(feature, wq[...], preferred_element_type=F32)
    new_forget = jnp.dot(feature, wf[...], preferred_element_type=F32)
    new_value = jnp.dot(feature, wv[...], preferred_element_type=F32).astype(BF16).astype(F32)
    new_gate = jnp.dot(feature, wo[...], preferred_element_type=F32)
    new_loss = floor_row * (1.0 / (1.0 + jnp.exp(new_forget)))
    read_weight = query * (1.0 - new_loss)
    sums[0] = query * new_loss
    sums[1] = new_value
    sums[2] = new_gate * (1.0 / (1.0 + jnp.exp(-new_gate)))
    seq = lax.broadcasted_iota(jnp.int32, read_weight.shape, 0)
    for a in range(2):
        picked = jnp.where(seq == prompt_of(place, a), read_weight, 0.0)
        sums[3 + a] = jnp.broadcast_to(jnp.sum(picked, axis=0, keepdims=True), read_weight.shape)

    def arrive(a, r):
        direct_in(a, r).wait_recv()
        for o in range(1, t):
            forward(a, r, o, core).start()

    def ready(a, r):
        if a == 0:
            keep_copy(r).wait_recv()
        for o in range(1, t):
            forward(a, r, o, lax.rem(core - o + t, t)).wait_recv()

    arrive(0, 1)
    for a in range(2):

        def step(r, carry, a=a):
            arrive(a, r)
            ready(a, r - 1)
            forget(a, r - 1)
            value(a, r - 1)
            return carry

        lax.fori_loop(2, members, step, 0)
        if a == 0:
            arrive(1, 1)
        ready(a, members - 1)
        forget(a, members - 1)
        finish(a)
    send_reads()

    mine = me // group
    source = member_of(lax.rem(mine, members))
    for z in range(planes):

        @pl.when(z * members + source != me)
        def _():
            pairs = [(got_totals.at[z], row_recv.at[z])]
            for b in range(batches):
                pairs.append((got_states.at[z, pl.ds(b * batch, batch)], state_recv.at[z, b]))
            for piece, arrived in pairs:
                pltpu.make_async_remote_copy(
                    src_ref=piece, dst_ref=piece,
                    send_sem=row_send.at[0, 0], recv_sem=arrived,
                    device_id=(z * members + source, core), device_id_type=MESH,
                ).wait_recv()

    first = lax.rem(me, group) * rows
    i0 = lax.broadcasted_iota(jnp.int32, (rows, head), 0) + first
    i1 = lax.broadcasted_iota(jnp.int32, (rows, head), 1)
    later = jnp.zeros((1, width), F32)
    final = [got_states[planes - 1, h] for h in range(heads)]
    for z in reversed(range(planes - 1)):
        later = later + got_totals[z + 1]
        decay = jnp.exp(later)
        for h in range(heads):
            row = jnp.broadcast_to(decay[:, h * head : (h + 1) * head], (rows, head))
            final[h] = final[h] + got_states[z, h] * jnp.sum(jnp.where(i0 == i1, row, 0.0), axis=1, keepdims=True)
    for h in range(heads):
        cache_out[h] = final[h].astype(BF16)

    for o in range(1, n):
        read_copy(o, lax.rem(me - o + n, n)).wait_recv()
    for s in range(s_count):
        row = jnp.zeros((1, width), F32)
        for z in range(planes):
            a = (s // members + 1 + (2 * z) // planes) % 2
            row = row + reads[z * members + member_of(s % members), a]
        sums[5, s : s + 1, :] = row
    for h in range(heads):
        lanes = slice(h * head, (h + 1) * head)
        mixed = sums[5, :, lanes] + jnp.sum(sums[0, :, lanes], axis=1, keepdims=True) * sums[1, :, lanes]
        normed = mixed * lax.rsqrt(jnp.mean(mixed * mixed, axis=1, keepdims=True) + EPSILON)
        read_out[:, lanes] = (normed * gain[...] * sums[2, :, lanes]).astype(BF16)

    for r in range(1, members):
        keep_copy(r).wait_send()
    for o in range(1, t):
        token_copy(o, core).wait_send()
    for a in range(2):
        for r in range(1, members):
            direct(a, r).wait_send()
            for o in range(1, t):
                forward(a, r, o, core).wait_send()
        for o in range(1, planes):
            total_copy(a, o, plane).wait_send()
        for g in range(group):

            @pl.when(keeper(a, g) != me)
            def _():
                row_copy(a, g).wait_send()
                for b in range(batches):
                    state_copy(a, g, b).wait_send()

    for o in range(1, n):
        read_copy(o, me).wait_send()


def per_device(prompt, keep_scale, new_token, w_query, w_forget, w_value, w_outgate, floor_gap, norm_gain):
    n, t = lax.axis_size("sp"), lax.axis_size("tp")
    s_count, positions, model = prompt.shape
    head = norm_gain.shape[0]
    width = w_forget.shape[1]
    heads = width // head
    members = s_count // 2
    planes = n // members
    group = n // s_count
    rows = head // group
    batches = 2 if heads % 2 == 0 else 1
    sizes = (n, t, s_count, members, group, heads, head, rows)
    dma = pltpu.SemaphoreType.DMA
    vmem = pl.BlockSpec(memory_space=pltpu.VMEM)
    hbm = pl.BlockSpec(memory_space=pl.ANY)
    return pl.pallas_call(
        functools.partial(kernel, sizes),
        out_shape=(
            jax.ShapeDtypeStruct((heads, rows, head), BF16),
            jax.ShapeDtypeStruct((s_count, width), BF16),
        ),
        in_specs=[hbm, vmem, vmem, hbm, hbm, hbm, hbm, vmem, vmem],
        out_specs=(vmem, vmem),
        scratch_shapes=[
            pltpu.VMEM((2, members, positions, model), BF16),
            pltpu.VMEM((members,) + keep_scale.shape, F32),
            pltpu.VMEM((t,) + new_token.shape, BF16),
            pltpu.VMEM((model, width), BF16),
            pltpu.VMEM((model, width), BF16),
            pltpu.VMEM((model, width), BF16),
            pltpu.VMEM((model, width), BF16),
            pltpu.VMEM((2, members, positions, width), F32),
            pltpu.VMEM((2, members, positions, width), BF16),
            pltpu.VMEM((2, members, width), F32),
            pltpu.VMEM((2, planes, 1, width), F32),
            pltpu.VMEM((planes, 1, width), F32),
            pltpu.VMEM((2, heads, head, head), F32),
            pltpu.VMEM((planes, heads, rows, head), F32),
            pltpu.VMEM((n, 2, 1, width), F32),
            pltpu.VMEM((6, s_count, width), F32),
            dma((6,)),
            dma((2, members)), dma((2, members)),
            dma((members,)), dma((members,)),
            dma((2, members, t)), dma((2, members, t)),
            dma((t,)), dma((t,)),
            dma((2, planes)), dma((2, planes)),
            dma((2, group)), dma((planes,)),
            dma((2, group, batches)), dma((planes, batches)),
            dma((n,)), dma((n,)),
        ],
        compiler_params=pltpu.CompilerParams(collective_id=0, has_side_effects=True),
    )(
        prompt, keep_scale, new_token, w_query, w_forget, w_value, w_outgate,
        floor_gap.reshape(1, width), norm_gain.reshape(1, head),
    )


def solution(mesh):
    return jax.shard_map(
        per_device,
        mesh=mesh,
        in_specs=(
            P(None, "sp", None),
            P(None, "sp"),
            P(None, "tp"),
            P(None, "tp"),
            P(None, "tp"),
            P(None, "tp"),
            P(None, "tp"),
            P("tp"),
            P(),
        ),
        out_specs=(P("tp", "sp", None), P(None, "tp")),
        check_vma=False,
    )
```

profile of v0, /device:TPU:0, one launch (start us, length us, event | category | flops | bytes accessed | tf_op | source)
XLA Modules:
  0.0 44.6 jit_solution(12949611180675967409)
XLA Ops:
  0.6 41.2 %shard_map.104 = (bf16[4,64,128]{2,1,0:T(8,128)(2,1)}, bf16[8,512]{1,0:T(8,128)(2,1)}) custom-call(bf16[8,64,2048]{2,1,0:T(8,128)(2,1)} %prompt.1, f32[8,64]{1,0:T(8,128)} %keep.1, bf16[8,1024]{1,0:T(8,128)(2,1)} %token_.1, bf16[2048,512]{1,0:T(8,128)(2,1)} %w_query.1, bf16[2048,512]{1,0:T(8,128)(2,1)} %w_forget.1, bf16[2048,512]{1,0:T(8,128)(2,1)} %w_value.1, ...), custom_call_target="tpu_custom_call" | custom-call | tf_op jit(solution)/shard_map/pallas_call | solution.py:390
  41.8 1.5 %copy.13 = bf16[4,64,128]{2,1,0:T(8,128)(2,1)} copy(bf16[4,64,128]{2,1,0:T(8,128)(2,1)} %get-tuple-element.4) | data formatting | bytes 131072
  43.3 1.3 %copy.14 = bf16[8,512]{1,0:T(8,128)(2,1)} copy(bf16[8,512]{1,0:T(8,128)(2,1)} %get-tuple-element.5) | data formatting | bytes 16384
where the time goes:
time: 44.9 us; the launch traced here: 44.6 us
  Pallas kernels  41.2 us (92%)
  local copies, waits for them, and re-layouts  2.77 us (6%)
  between operations  0.64 us (1%)
    pallas_call x1, Pallas kernels, per_device(): pl.pallas_call(functools.partial(kernel, sizes), out_shape=(jax.ShapeDtyp...  41.2 us
    unnamed x2, local copies, waits for them, and re-layouts  2.77 us

commit v1 on v0

v1 whole, which is shorter than its diff:
```python
import functools

import jax
import jax.numpy as jnp
from jax import lax
from jax.experimental import pallas as pl
from jax.experimental.pallas import tpu as pltpu
from jax.sharding import PartitionSpec as P

EPSILON = 1e-06
MESH = pl.DeviceIdType.MESH
F32 = jnp.float32
BF16 = jnp.bfloat16


def partner(mine, step, count):
    total, bit = 0, 1
    while bit < count:
        total = total + bit * lax.rem(lax.rem(mine // bit, 2) + lax.rem(step // bit, 2), 2)
        bit *= 2
    return total


def pieces(x, count):
    out = []
    for _ in range(count):
        piece = x.astype(BF16)
        out.append(piece)
        x = x - piece.astype(F32)
    return out


def arrival_order(members):
    if members == 8:
        return (0, 7, 3, 4, 5, 2, 6, 1)
    return (0,) + tuple(range(members - 1, 0, -1))


def kernel(
    sizes,
    prompt, keep, token, w_query, w_forget, w_value, w_outgate, floor, gain,
    cache_out, read_out,
    stage, blocks, keeps, tokens, wq, wf, wv, wo, floors, gains,
    weighted, values, logs, suffixes, decays, totals, got_totals, states, got_states, reads, sums,
    local_sem, stage_sem, direct_send, direct_recv, keep_send, keep_recv, fwd_send, fwd_recv,
    token_send, token_recv, total_send, total_recv, row_send, row_recv, state_send, state_recv, read_send, read_recv,
):
    n, t, s_count, members, cubes, heads, head, rows = sizes
    group = cubes
    me, core = lax.axis_index("sp"), lax.axis_index("tp")
    cube, place = me // members, lax.rem(me, members)
    model = prompt.shape[2]
    part = model // t
    positions = prompt.shape[1]
    width = heads * head
    order = arrival_order(members)
    pairs = members // 2
    batches = 2 if heads % 2 == 0 else 1
    batch = heads // batches

    def prompt_of(p):
        if members % 4:
            return p
        low = lax.rem(p, 4)
        return p - low + lax.rem(low, 2) * 2 + low // 2

    def columns(c):
        return pl.ds(pl.multiple_of(c * part, part), part)

    def relation(k):
        if isinstance(k, int):
            return order[k]
        r = 0
        for i, value in enumerate(order):
            r = r + value * jnp.where(k == i, 1, 0)
        return r

    def peer(k):
        return partner(place, relation(k), members)

    mine = prompt_of(place)

    staged = [None] + [
        pltpu.make_async_copy(prompt.at[prompt_of(peer(k)), :, columns(core)], stage.at[k - 1], stage_sem.at[k])
        for k in range(1, members)
    ]
    local = [
        pltpu.make_async_copy(keep, keeps.at[0], local_sem.at[0]),
        pltpu.make_async_copy(token, tokens.at[core], local_sem.at[1]),
        pltpu.make_async_copy(floor, floors, local_sem.at[2]),
        pltpu.make_async_copy(gain, gains, local_sem.at[3]),
        pltpu.make_async_copy(prompt.at[mine], blocks.at[0], local_sem.at[4]),
        pltpu.make_async_copy(w_forget, wf, local_sem.at[5]),
        pltpu.make_async_copy(w_value, wv, local_sem.at[6]),
        pltpu.make_async_copy(w_query, wq, local_sem.at[7]),
        pltpu.make_async_copy(w_outgate, wo, local_sem.at[8]),
    ]

    barrier = pltpu.get_barrier_semaphore()
    for k in range(1, members):
        pl.semaphore_signal(barrier, inc=1, device_id=(cube * members + peer(k), core), device_id_type=MESH)
    for o in range(1, cubes):
        pl.semaphore_signal(barrier, inc=1, device_id=(lax.rem(me + o * members, n), core), device_id_type=MESH)
    for o in range(1, t):
        pl.semaphore_signal(barrier, inc=1, device_id=(me, lax.rem(core + o, t)), device_id_type=MESH)
    local[0].start()
    local[1].start()
    for k in range(1, members):
        staged[k].start()
    for copy in local[2:]:
        copy.start()

    def direct(k):
        return pltpu.make_async_remote_copy(
            src_ref=stage.at[k - 1],
            dst_ref=blocks.at[k, :, columns(core)],
            send_sem=direct_send.at[k], recv_sem=direct_recv.at[k],
            device_id=(cube * members + peer(k), core), device_id_type=MESH,
        )

    def keep_copy(k):
        return pltpu.make_async_remote_copy(
            src_ref=keeps.at[0], dst_ref=keeps.at[k],
            send_sem=keep_send.at[k], recv_sem=keep_recv.at[k],
            device_id=(cube * members + peer(k), core), device_id_type=MESH,
        )

    def forward(k, o, c):
        piece = blocks.at[k, :, columns(c)]
        return pltpu.make_async_remote_copy(
            src_ref=piece, dst_ref=piece,
            send_sem=fwd_send.at[k, o], recv_sem=fwd_recv.at[k, o],
            device_id=(me, lax.rem(core + o, t)), device_id_type=MESH,
        )

    def token_copy(o, c):
        return pltpu.make_async_remote_copy(
            src_ref=tokens.at[c], dst_ref=tokens.at[c],
            send_sem=token_send.at[o], recv_sem=token_recv.at[o],
            device_id=(me, lax.rem(core + o, t)), device_id_type=MESH,
        )

    local[0].wait()
    local[1].wait()
    with jax.named_scope("barrier"):
        pl.semaphore_wait(barrier, members - 1 + cubes - 1 + t - 1)
    for k in range(1, members):
        keep_copy(k).start()
    for k in range(1, members):
        staged[k].wait()
        direct(k).start()
    for o in range(1, t):
        token_copy(o, core).start()

    with jax.named_scope("wlocal"):
        for copy in local[2:]:
            copy.wait()
        for o in range(1, t):
            token_copy(o, lax.rem(core - o + t, t)).wait_recv()
    floor_row = floors[...]

    with jax.named_scope("token"):
        feature = jnp.concatenate([tokens[c] for c in range(t)], axis=1)
        query = jnp.dot(feature, wq[...], preferred_element_type=F32)
        new_forget = jnp.dot(feature, wf[...], preferred_element_type=F32)
        new_value = jnp.dot(feature, wv[...], preferred_element_type=F32).astype(BF16).astype(F32)
        new_gate = jnp.dot(feature, wo[...], preferred_element_type=F32)
        new_loss = floor_row * (1.0 / (1.0 + jnp.exp(new_forget)))
        read_weight = query * (1.0 - new_loss)
        sums[0] = query * new_loss
        sums[1] = new_value
        sums[2] = new_gate * (1.0 / (1.0 + jnp.exp(-new_gate)))
        seq = lax.broadcasted_iota(jnp.int32, read_weight.shape, 0)
        picked = jnp.where(seq == mine, read_weight, 0.0)
        sums[3] = jnp.broadcast_to(jnp.sum(picked, axis=0, keepdims=True), read_weight.shape)

    def block_rows(k, count):
        return blocks[pl.ds(k, count)].reshape(count * positions, model)

    def value(k, count):
        out = jnp.dot(block_rows(k, count), wv[...], preferred_element_type=F32).astype(BF16)
        values[pl.ds(k, count)] = out.reshape(count, positions, width)

    def forget(k, count):
        size = count * positions
        pre = jnp.dot(block_rows(k, count), wf[...], preferred_element_type=F32)
        loss = floor_row * (1.0 / (1.0 + jnp.exp(pre)))
        i0 = lax.broadcasted_iota(jnp.int32, (positions, positions), 0)
        i1 = lax.broadcasted_iota(jnp.int32, (positions, positions), 1)
        scale = []
        for i in range(count):
            row = jnp.broadcast_to(keeps[k + i, pl.ds(mine, 1), :], (positions, positions))
            scale.append(jnp.sum(jnp.where(i0 == i1, row, 0.0), axis=1, keepdims=True))
        scale = jnp.concatenate(scale, axis=0)
        log_forget = jnp.log(scale) + jnp.log1p(-loss)
        gate = 1.0 - scale + scale * loss
        j0 = lax.broadcasted_iota(jnp.int32, (size, size), 0)
        j1 = lax.broadcasted_iota(jnp.int32, (size, size), 1)
        later = jnp.where((j1 > j0) & (j0 // positions == j1 // positions), 1.0, 0.0).astype(BF16)
        inside = sum(jnp.dot(later, piece, preferred_element_type=F32) for piece in pieces(log_forget, 3))
        for i in range(count):
            first = i * positions
            logs[pl.ds(peer(k + i), 1), :] = inside[first : first + 1] + log_forget[first : first + 1]
        weighted[pl.ds(k, count)] = (gate * jnp.exp(inside)).reshape(count, positions, width)

    def arrive(k):
        with jax.named_scope("w_direct"):
            direct(k).wait_recv()
        for o in range(1, t):
            forward(k, o, core).start()

    def ready(k):
        with jax.named_scope("w_fwd"):
            keep_copy(k).wait_recv()
            for o in range(1, t):
                forward(k, o, lax.rem(core - o + t, t)).wait_recv()

    arrive(1)
    for j in range(pairs):
        if j < pairs - 1:
            arrive(2 * j + 2)
            arrive(2 * j + 3)
        if j > 0:
            ready(2 * j)
        ready(2 * j + 1)
        with jax.named_scope("forget"):
            forget(2 * j, 2)
        if j < pairs - 1:
            with jax.named_scope("value"):
                value(2 * j, 2)

    def total_copy(o, c):
        return pltpu.make_async_remote_copy(
            src_ref=totals.at[c], dst_ref=totals.at[c],
            send_sem=total_send.at[o], recv_sem=total_recv.at[o],
            device_id=(lax.rem(me + o * members, n), core), device_id_type=MESH,
        )

    def keeper(g):
        return mine * group + g

    def row_copy(g):
        return pltpu.make_async_remote_copy(
            src_ref=totals.at[cube], dst_ref=got_totals.at[cube],
            send_sem=row_send.at[g], recv_sem=row_recv.at[cube],
            device_id=(keeper(g), core), device_id_type=MESH,
        )

    def state_copy(g, b):
        return pltpu.make_async_remote_copy(
            src_ref=states.at[pl.ds(b * batch, batch), pl.ds(g * rows, rows), :],
            dst_ref=got_states.at[cube, pl.ds(b * batch, batch)],
            send_sem=state_send.at[g, b], recv_sem=state_recv.at[cube, b],
            device_id=(keeper(g), core), device_id_type=MESH,
        )

    def read_copy(o, sender):
        return pltpu.make_async_remote_copy(
            src_ref=reads.at[sender], dst_ref=reads.at[sender],
            send_sem=read_send.at[o], recv_sem=read_recv.at[o],
            device_id=(lax.rem(me + o, n), core), device_id_type=MESH,
        )

    def make_states(b):
        for h in range(b * batch, (b + 1) * batch):
            lanes = slice(h * head, (h + 1) * head)
            w = jnp.concatenate([weighted[k, :, lanes] * decays[k : k + 1, lanes] for k in range(members)], axis=0)
            v = values[:, :, lanes].reshape(members * positions, head)
            states[h] = sum(
                lax.dot_general(piece, v, (((0,), (0,)), ((), ())), preferred_element_type=F32)
                for piece in pieces(w, 2)
            )

    def send_states(b):
        for g in range(group):

            @pl.when(keeper(g) != me)
            def _():
                state_copy(g, b).start()

            @pl.when(keeper(g) == me)
            def _():
                got_states[cube, b * batch : (b + 1) * batch] = states[b * batch : (b + 1) * batch, g * rows : (g + 1) * rows, :]

    with jax.named_scope("finish"):
        suffix = jnp.zeros((1, width), F32)
        for p in reversed(range(members)):
            suffixes[p : p + 1, :] = suffix
            suffix = suffix + logs[p : p + 1, :]
        totals[cube] = suffix
        for o in range(1, cubes):
            total_copy(o, cube).start()
        for g in range(group):

            @pl.when(keeper(g) != me)
            def _():
                row_copy(g).start()

            @pl.when(keeper(g) == me)
            def _():
                got_totals[cube] = suffix

        value(members - 2, 2)
        for k in range(members):
            decays[k : k + 1, :] = jnp.exp(suffixes[pl.ds(peer(k), 1), :])
        make_states(0)
        send_states(0)
        for b in range(1, batches):
            make_states(b)
    with jax.named_scope("w_totals"):
        for o in range(1, cubes):
            total_copy(o, lax.rem(cube - o + cubes, cubes)).wait_recv()
    with jax.named_scope("sendreads"):
        later = jnp.zeros((1, width), F32)
        for c in range(cubes):
            later = later + jnp.where(c > cube, totals[c], 0.0)
        decay = jnp.exp(later)
        for h in range(heads):
            lanes = slice(h * head, (h + 1) * head)
            reads[me, :, lanes] = jnp.dot(
                sums[3, :, lanes] * decay[:, lanes], states[h],
                preferred_element_type=F32, precision=lax.Precision.HIGHEST,
            )[0:1]
        for o in range(n - 1, 0, -1):
            read_copy(o, me).start()
        for b in range(1, batches):
            send_states(b)

    source = prompt_of(me // group)
    for c in range(cubes):

        @pl.when(c * members + source != me)
        @jax.named_scope("w_states")
        def _():
            arrivals = [(got_totals.at[c], row_recv.at[c])]
            for b in range(batches):
                arrivals.append((got_states.at[c, pl.ds(b * batch, batch)], state_recv.at[c, b]))
            for piece, arrived in arrivals:
                pltpu.make_async_remote_copy(
                    src_ref=piece, dst_ref=piece,
                    send_sem=row_send.at[0], recv_sem=arrived,
                    device_id=(c * members + source, core), device_id_type=MESH,
                ).wait_recv()

    first = lax.rem(me, group) * rows
    i0 = lax.broadcasted_iota(jnp.int32, (rows, head), 0) + first
    i1 = lax.broadcasted_iota(jnp.int32, (rows, head), 1)
    later = jnp.zeros((1, width), F32)
    final = [got_states[cubes - 1, h] for h in range(heads)]
    for c in reversed(range(cubes - 1)):
        later = later + got_totals[c + 1]
        decay = jnp.exp(later)
        for h in range(heads):
            row = jnp.broadcast_to(decay[:, h * head : (h + 1) * head], (rows, head))
            final[h] = final[h] + got_states[c, h] * jnp.sum(jnp.where(i0 == i1, row, 0.0), axis=1, keepdims=True)
    for h in range(heads):
        cache_out[h] = final[h].astype(BF16)

    with jax.named_scope("w_reads"):
        for o in range(1, n):
            read_copy(o, lax.rem(me - o + n, n)).wait_recv()
    for s in range(s_count):
        row = jnp.zeros((1, width), F32)
        for c in range(cubes):
            row = row + reads[c * members + prompt_of(s)]
        sums[4, s : s + 1, :] = row
    for h in range(heads):
        lanes = slice(h * head, (h + 1) * head)
        mixed = sums[4, :, lanes] + jnp.sum(sums[0, :, lanes], axis=1, keepdims=True) * sums[1, :, lanes]
        normed = mixed * lax.rsqrt(jnp.mean(mixed * mixed, axis=1, keepdims=True) + EPSILON)
        read_out[:, lanes] = (normed * gains[...] * sums[2, :, lanes]).astype(BF16)

    with jax.named_scope("w_sends"):
        for k in range(1, members):
            keep_copy(k).wait_send()
            direct(k).wait_send()
            for o in range(1, t):
                forward(k, o, core).wait_send()
        for o in range(1, t):
            token_copy(o, core).wait_send()
        for o in range(1, cubes):
            total_copy(o, cube).wait_send()
        for g in range(group):

            @pl.when(keeper(g) != me)
            def _():
                row_copy(g).wait_send()
                for b in range(batches):
                    state_copy(g, b).wait_send()

        for o in range(1, n):
            read_copy(o, me).wait_send()


def per_device(prompt, keep_scale, new_token, w_query, w_forget, w_value, w_outgate, floor_gap, norm_gain):
    n, t = lax.axis_size("sp"), lax.axis_size("tp")
    s_count, positions, model = prompt.shape
    head = norm_gain.shape[0]
    width = w_forget.shape[1]
    heads = width // head
    members = s_count
    cubes = n // members
    group = cubes
    rows = head // group
    batches = 2 if heads % 2 == 0 else 1
    sizes = (n, t, s_count, members, cubes, heads, head, rows)
    dma = pltpu.SemaphoreType.DMA
    vmem = pl.BlockSpec(memory_space=pltpu.VMEM)
    hbm = pl.BlockSpec(memory_space=pl.ANY)
    return pl.pallas_call(
        functools.partial(kernel, sizes),
        out_shape=(
            jax.ShapeDtypeStruct((heads, rows, head), BF16),
            jax.ShapeDtypeStruct((s_count, width), BF16),
        ),
        in_specs=[hbm] * 9,
        out_specs=(vmem, vmem),
        scratch_shapes=[
            pltpu.VMEM((members - 1, positions, model // t), BF16),
            pltpu.VMEM((members, positions, model), BF16),
            pltpu.VMEM((members,) + keep_scale.shape, F32),
            pltpu.VMEM((t,) + new_token.shape, BF16),
            pltpu.VMEM((model, width), BF16),
            pltpu.VMEM((model, width), BF16),
            pltpu.VMEM((model, width), BF16),
            pltpu.VMEM((model, width), BF16),
            pltpu.VMEM((1, width), F32),
            pltpu.VMEM((1, head), F32),
            pltpu.VMEM((members, positions, width), F32),
            pltpu.VMEM((members, positions, width), BF16),
            pltpu.VMEM((members, width), F32),
            pltpu.VMEM((members, width), F32),
            pltpu.VMEM((members, width), F32),
            pltpu.VMEM((cubes, 1, width), F32),
            pltpu.VMEM((cubes, 1, width), F32),
            pltpu.VMEM((heads, head, head), F32),
            pltpu.VMEM((cubes, heads, rows, head), F32),
            pltpu.VMEM((n, 1, width), F32),
            pltpu.VMEM((5, s_count, width), F32),
            dma((9,)),
            dma((members,)),
            dma((members,)), dma((members,)),
            dma((members,)), dma((members,)),
            dma((members, t)), dma((members, t)),
            dma((t,)), dma((t,)),
            dma((cubes,)), dma((cubes,)),
            dma((group,)), dma((cubes,)),
            dma((group, batches)), dma((cubes, batches)),
            dma((n,)), dma((n,)),
        ],
        compiler_params=pltpu.CompilerParams(collective_id=0, has_side_effects=True),
    )(
        prompt, keep_scale, new_token, w_query, w_forget, w_value, w_outgate,
        floor_gap.reshape(1, width), norm_gain.reshape(1, head),
    )


def solution(mesh):
    return jax.shard_map(
        per_device,
        mesh=mesh,
        in_specs=(
            P(None, "sp", None),
            P(None, "sp"),
            P(None, "tp"),
            P(None, "tp"),
            P(None, "tp"),
            P(None, "tp"),
            P(None, "tp"),
            P("tp"),
            P(),
        ),
        out_specs=(P("tp", "sp", None), P(None, "tp")),
        check_vma=False,
    )
```

time: 44.9 us -> 35.7 us (0.80)
  Pallas kernels: 41.2 us -> 32.1 us
    pallas_call x1, Pallas kernels: 41.2 us -> 32.1 us  [per_device(): pl.pallas_call(functools.partial(kernel, sizes), out_shape=(jax.ShapeDtyp...]
where the time goes in v1:
time: 35.7 us; the launch traced here: 35.5 us
  Pallas kernels  32.1 us (90%)
  local copies, waits for them, and re-layouts  2.77 us (8%)
  between operations  0.64 us (2%)
    pallas_call x1, Pallas kernels, per_device(): pl.pallas_call(functools.partial(kernel, sizes), out_shape=(jax.ShapeDtyp...  32.1 us
    unnamed x2, local copies, waits for them, and re-layouts  2.77 us

profile of v1, /device:TPU:0, one launch (start us, length us, event | category | flops | bytes accessed | tf_op | source)
XLA Modules:
  0.0 35.5 jit_solution(740032863618156794)
XLA Ops:
  0.6 32.1 %shard_map.104 = (bf16[4,64,128]{2,1,0:T(8,128)(2,1)}, bf16[8,512]{1,0:T(8,128)(2,1)}) custom-call(bf16[8,64,2048]{2,1,0:T(8,128)(2,1)} %prompt.1, f32[8,64]{1,0:T(8,128)} %keep.1, bf16[8,1024]{1,0:T(8,128)(2,1)} %token_.1, bf16[2048,512]{1,0:T(8,128)(2,1)} %w_query.1, bf16[2048,512]{1,0:T(8,128)(2,1)} %w_forget.1, bf16[2048,512]{1,0:T(8,128)(2,1)} %w_value.1, ...), custom_call_target="tpu_custom_call" | custom-call | tf_op jit(solution)/shard_map/pallas_call | solution.py:410
  32.7 1.5 %copy.13 = bf16[4,64,128]{2,1,0:T(8,128)(2,1)} copy(bf16[4,64,128]{2,1,0:T(8,128)(2,1)} %get-tuple-element.4) | data formatting | bytes 131072
  34.2 1.3 %copy.14 = bf16[8,512]{1,0:T(8,128)(2,1)} copy(bf16[8,512]{1,0:T(8,128)(2,1)} %get-tuple-element.5) | data formatting | bytes 16384

commit v2 on v1

--- a/solution.py
+++ b/solution.py
@@ -14,9 +14,10 @@
 
 
 def partner(mine, step, count):
-    total, bit = 0, 1
+    total, bit = mine, 1
     while bit < count:
-        total = total + bit * lax.rem(lax.rem(mine // bit, 2) + lax.rem(step // bit, 2), 2)
+        if step // bit % 2:
+            total = total + bit * (1 - 2 * lax.rem(mine // bit, 2))
         bit *= 2
     return total
 
@@ -67,21 +68,15 @@
     def columns(c):
         return pl.ds(pl.multiple_of(c * part, part), part)
 
-    def relation(k):
-        if isinstance(k, int):
-            return order[k]
-        r = 0
-        for i, value in enumerate(order):
-            r = r + value * jnp.where(k == i, 1, 0)
-        return r
+    peers = [partner(place, r, members) for r in order]
 
     def peer(k):
-        return partner(place, relation(k), members)
+        return peers[k]
 
     mine = prompt_of(place)
 
     staged = [None] + [
-        pltpu.make_async_copy(prompt.at[prompt_of(peer(k)), :, columns(core)], stage.at[k - 1], stage_sem.at[k])
+        pltpu.make_async_copy(prompt.at[prompt_of(peer(k)), :, columns(core)], stage.at[k - 1], stage_sem.at[k - 1])
         for k in range(1, members)
     ]
     local = [
@@ -96,6 +91,10 @@
         pltpu.make_async_copy(w_outgate, wo, local_sem.at[8]),
     ]
 
+    for k in range(1, members):
+        staged[k].start()
+    local[0].start()
+    local[1].start()
     barrier = pltpu.get_barrier_semaphore()
     for k in range(1, members):
         pl.semaphore_signal(barrier, inc=1, device_id=(cube * members + peer(k), core), device_id_type=MESH)
@@ -103,10 +102,6 @@
         pl.semaphore_signal(barrier, inc=1, device_id=(lax.rem(me + o * members, n), core), device_id_type=MESH)
     for o in range(1, t):
         pl.semaphore_signal(barrier, inc=1, device_id=(me, lax.rem(core + o, t)), device_id_type=MESH)
-    local[0].start()
-    local[1].start()
-    for k in range(1, members):
-        staged[k].start()
     for copy in local[2:]:
         copy.start()
 
@@ -114,14 +109,14 @@
         return pltpu.make_async_remote_copy(
             src_ref=stage.at[k - 1],
             dst_ref=blocks.at[k, :, columns(core)],
-            send_sem=direct_send.at[k], recv_sem=direct_recv.at[k],
+            send_sem=direct_send, recv_sem=direct_recv.at[k - 1],
             device_id=(cube * members + peer(k), core), device_id_type=MESH,
         )
 
     def keep_copy(k):
         return pltpu.make_async_remote_copy(
             src_ref=keeps.at[0], dst_ref=keeps.at[k],
-            send_sem=keep_send.at[k], recv_sem=keep_recv.at[k],
+            send_sem=keep_send, recv_sem=keep_recv,
             device_id=(cube * members + peer(k), core), device_id_type=MESH,
         )
 
@@ -129,14 +124,14 @@
         piece = blocks.at[k, :, columns(c)]
         return pltpu.make_async_remote_copy(
             src_ref=piece, dst_ref=piece,
-            send_sem=fwd_send.at[k, o], recv_sem=fwd_recv.at[k, o],
+            send_sem=fwd_send.at[o - 1], recv_sem=fwd_recv.at[k - 1, o - 1],
             device_id=(me, lax.rem(core + o, t)), device_id_type=MESH,
         )
 
     def token_copy(o, c):
         return pltpu.make_async_remote_copy(
             src_ref=tokens.at[c], dst_ref=tokens.at[c],
-            send_sem=token_send.at[o], recv_sem=token_recv.at[o],
+            send_sem=token_send.at[o - 1], recv_sem=token_recv.at[o - 1],
             device_id=(me, lax.rem(core + o, t)), device_id_type=MESH,
         )
 
@@ -192,12 +187,12 @@
             row = jnp.broadcast_to(keeps[k + i, pl.ds(mine, 1), :], (positions, positions))
             scale.append(jnp.sum(jnp.where(i0 == i1, row, 0.0), axis=1, keepdims=True))
         scale = jnp.concatenate(scale, axis=0)
-        log_forget = jnp.log(scale) + jnp.log1p(-loss)
+        log_forget = jnp.log(scale * (1.0 - loss))
         gate = 1.0 - scale + scale * loss
         j0 = lax.broadcasted_iota(jnp.int32, (size, size), 0)
         j1 = lax.broadcasted_iota(jnp.int32, (size, size), 1)
         later = jnp.where((j1 > j0) & (j0 // positions == j1 // positions), 1.0, 0.0).astype(BF16)
-        inside = sum(jnp.dot(later, piece, preferred_element_type=F32) for piece in pieces(log_forget, 3))
+        inside = sum(jnp.dot(later, piece, preferred_element_type=F32) for piece in pieces(log_forget, 2))
         for i in range(count):
             first = i * positions
             logs[pl.ds(peer(k + i), 1), :] = inside[first : first + 1] + log_forget[first : first + 1]
@@ -211,11 +206,22 @@
 
     def ready(k):
         with jax.named_scope("w_fwd"):
-            keep_copy(k).wait_recv()
             for o in range(1, t):
                 forward(k, o, lax.rem(core - o + t, t)).wait_recv()
 
+    def many(ref, send, recv):
+        return pltpu.make_async_remote_copy(
+            src_ref=ref, dst_ref=ref, send_sem=send, recv_sem=recv,
+            device_id=(lax.rem(me + 1, n), core), device_id_type=MESH,
+        )
+
+    all_keeps = many(keeps.at[pl.ds(1, members - 1)], keep_send, keep_recv)
+    all_direct = many(stage, direct_send, direct_recv.at[0])
+    all_totals = many(totals.at[pl.ds(0, cubes - 1)], total_send, total_recv)
+    all_reads = many(reads.at[pl.ds(0, n - 1)], read_send, read_recv)
+
     arrive(1)
+    all_keeps.wait_recv()
     for j in range(pairs):
         if j < pairs - 1:
             arrive(2 * j + 2)
@@ -232,7 +238,7 @@
     def total_copy(o, c):
         return pltpu.make_async_remote_copy(
             src_ref=totals.at[c], dst_ref=totals.at[c],
-            send_sem=total_send.at[o], recv_sem=total_recv.at[o],
+            send_sem=total_send, recv_sem=total_recv,
             device_id=(lax.rem(me + o * members, n), core), device_id_type=MESH,
         )
 
@@ -250,14 +256,14 @@
         return pltpu.make_async_remote_copy(
             src_ref=states.at[pl.ds(b * batch, batch), pl.ds(g * rows, rows), :],
             dst_ref=got_states.at[cube, pl.ds(b * batch, batch)],
-            send_sem=state_send.at[g, b], recv_sem=state_recv.at[cube, b],
+            send_sem=state_send.at[g], recv_sem=state_recv.at[cube],
             device_id=(keeper(g), core), device_id_type=MESH,
         )
 
     def read_copy(o, sender):
         return pltpu.make_async_remote_copy(
             src_ref=reads.at[sender], dst_ref=reads.at[sender],
-            send_sem=read_send.at[o], recv_sem=read_recv.at[o],
+            send_sem=read_send, recv_sem=read_recv,
             device_id=(lax.rem(me + o, n), core), device_id_type=MESH,
         )
 
@@ -308,8 +314,7 @@
         for b in range(1, batches):
             make_states(b)
     with jax.named_scope("w_totals"):
-        for o in range(1, cubes):
-            total_copy(o, lax.rem(cube - o + cubes, cubes)).wait_recv()
+        all_totals.wait_recv()
     with jax.named_scope("sendreads"):
         later = jnp.zeros((1, width), F32)
         for c in range(cubes):
@@ -332,10 +337,7 @@
         @pl.when(c * members + source != me)
         @jax.named_scope("w_states")
         def _():
-            arrivals = [(got_totals.at[c], row_recv.at[c])]
-            for b in range(batches):
-                arrivals.append((got_states.at[c, pl.ds(b * batch, batch)], state_recv.at[c, b]))
-            for piece, arrived in arrivals:
+            for piece, arrived in ((got_totals.at[c], row_recv.at[c]), (got_states.at[c], state_recv.at[c])):
                 pltpu.make_async_remote_copy(
                     src_ref=piece, dst_ref=piece,
                     send_sem=row_send.at[0], recv_sem=arrived,
@@ -357,8 +359,7 @@
         cache_out[h] = final[h].astype(BF16)
 
     with jax.named_scope("w_reads"):
-        for o in range(1, n):
-            read_copy(o, lax.rem(me - o + n, n)).wait_recv()
+        all_reads.wait_recv()
     for s in range(s_count):
         row = jnp.zeros((1, width), F32)
         for c in range(cubes):
@@ -370,26 +371,28 @@
         normed = mixed * lax.rsqrt(jnp.mean(mixed * mixed, axis=1, keepdims=True) + EPSILON)
         read_out[:, lanes] = (normed * gains[...] * sums[2, :, lanes]).astype(BF16)
 
-    with jax.named_scope("w_sends"):
-        for k in range(1, members):
-            keep_copy(k).wait_send()
-            direct(k).wait_send()
-            for o in range(1, t):
-                forward(k, o, core).wait_send()
-        for o in range(1, t):
-            token_copy(o, core).wait_send()
-        for o in range(1, cubes):
-            total_copy(o, cube).wait_send()
-        for g in range(group):
-
-            @pl.when(keeper(g) != me)
-            def _():
-                row_copy(g).wait_send()
-                for b in range(batches):
-                    state_copy(g, b).wait_send()
-
-        for o in range(1, n):
-            read_copy(o, me).wait_send()
+    all_keeps.wait_send()
+    all_direct.wait_send()
+    for o in range(1, t):
+        token_copy(o, core).wait_send()
+        many(blocks.at[pl.ds(1, members - 1), :, columns(core)], fwd_send.at[o - 1], read_recv).wait_send()
+    all_totals.wait_send()
+    for g in range(group):
+
+        @pl.when(keeper(g) != me)
+        def _():
+            row_copy(g).wait_send()
+            many(states.at[:, pl.ds(g * rows, rows), :], state_send.at[g], read_recv).wait_send()
+
+    all_reads.wait_send()
+
+
+def hand_over(cache, read, cache_out, read_out, sem):
+    copies = [pltpu.make_async_copy(cache, cache_out, sem.at[0]), pltpu.make_async_copy(read, read_out, sem.at[1])]
+    for copy in copies:
+        copy.start()
+    for copy in copies:
+        copy.wait()
 
 
 def per_device(prompt, keep_scale, new_token, w_query, w_forget, w_value, w_outgate, floor_gap, norm_gain):
@@ -406,12 +409,12 @@
     sizes = (n, t, s_count, members, cubes, heads, head, rows)
     dma = pltpu.SemaphoreType.DMA
     vmem = pl.BlockSpec(memory_space=pltpu.VMEM)
-    hbm = pl.BlockSpec(memory_space=pl.ANY)
-    return pl.pallas_call(
+    hbm = pl.BlockSpec(memory_space=pltpu.HBM)
+    cache, read = pl.pallas_call(
         functools.partial(kernel, sizes),
         out_shape=(
-            jax.ShapeDtypeStruct((heads, rows, head), BF16),
-            jax.ShapeDtypeStruct((s_count, width), BF16),
+            pltpu.VMEM((heads, rows, head), BF16),
+            pltpu.VMEM((s_count, width), BF16),
         ),
         in_specs=[hbm] * 9,
         out_specs=(vmem, vmem),
@@ -437,22 +440,37 @@
             pltpu.VMEM((cubes, heads, rows, head), F32),
             pltpu.VMEM((n, 1, width), F32),
             pltpu.VMEM((5, s_count, width), F32),
-            dma((9,)),
-            dma((members,)),
-            dma((members,)), dma((members,)),
-            dma((members,)), dma((members,)),
-            dma((members, t)), dma((members, t)),
-            dma((t,)), dma((t,)),
-            dma((cubes,)), dma((cubes,)),
+            dma((9,)), dma((members - 1,)),
+            dma, dma((members - 1,)),
+            dma, dma,
+            dma((t - 1,)), dma((members - 1, t - 1)),
+            dma((t - 1,)), dma((t - 1,)),
+            dma, dma,
             dma((group,)), dma((cubes,)),
-            dma((group, batches)), dma((cubes, batches)),
-            dma((n,)), dma((n,)),
+            dma((group,)), dma((cubes,)),
+            dma, dma,
         ],
-        compiler_params=pltpu.CompilerParams(collective_id=0, has_side_effects=True),
+        compiler_params=pltpu.CompilerParams(collective_id=0, has_side_effects=True, vmem_limit_bytes=32*1024*1024),
     )(
-        prompt, keep_scale, new_token, w_query, w_forget, w_value, w_outgate,
-        floor_gap.reshape(1, width), norm_gain.reshape(1, head),
+        *(
+            pltpu.with_memory_space_constraint(x, pltpu.HBM)
+            for x in (
+                prompt, keep_scale, new_token, w_query, w_forget, w_value, w_outgate,
+                floor_gap.reshape(1, width), norm_gain.reshape(1, head),
+            )
+        )
     )
+    return pl.pallas_call(
+        hand_over,
+        out_shape=(
+            jax.ShapeDtypeStruct((heads, rows, head), BF16),
+            jax.ShapeDtypeStruct((s_count, width), BF16),
+        ),
+        in_specs=[vmem, vmem],
+        out_specs=(pl.BlockSpec(memory_space=pltpu.HBM), pl.BlockSpec(memory_space=pltpu.HBM)),
+        scratch_shapes=[dma((2,))],
+        compiler_params=pltpu.CompilerParams(vmem_limit_bytes=1024*1024),
+    )(cache, read)
 
 
 def solution(mesh):

time: 35.7 us -> 32 us (0.90)
  local copies, waits for them, and re-layouts: 2.77 us -> 0 us
  Pallas kernels: 32.1 us -> 31.2 us
    unnamed x2 -> x0, local copies, waits for them, and re-layouts: 2.77 us -> none
    pallas_call x1 -> x2, Pallas kernels: 32.1 us -> 31.2 us  [the longest x1 30.5 us: per_device(): pl.pallas_call(functools.partial(kernel, sizes), out_shape=(pltpu.VMEM((h...]
where the time goes in v2:
time: 32 us; the launch traced here: 31.8 us
  Pallas kernels  31.2 us (98%)
  between operations  0.64 us (2%)
    pallas_call x1, Pallas kernels, per_device(): pl.pallas_call(functools.partial(kernel, sizes), out_shape=(pltpu.VMEM((h...  30.5 us
    pallas_call x1, Pallas kernels, per_device(): pl.pallas_call(hand_over, out_shape=(jax.ShapeDtypeStruct((heads, rows, h...  0.65 us

profile of v2, /device:TPU:0, one launch (start us, length us, event | category | flops | bytes accessed | tf_op | source)
XLA Modules:
  0.0 31.8 jit_solution(7272902909769756766)
XLA Ops:
  0.6 30.5 %shard_map.104 = (bf16[4,64,128]{2,1,0:T(8,128)(2,1)S(1)}, bf16[8,512]{1,0:T(8,128)(2,1)S(1)}) custom-call(bf16[8,64,2048]{2,1,0:T(8,128)(2,1)} %prompt.1, f32[8,64]{1,0:T(8,128)} %keep.1, bf16[8,1024]{1,0:T(8,128)(2,1)} %token_.1, bf16[2048,512]{1,0:T(8,128)(2,1)} %w_query.1, bf16[2048,512]{1,0:T(8,128)(2,1)} %w_forget.1, bf16[2048,512]{1,0:T(8,128)(2,1)} %w_value.1, ...), custom_call_target="tpu_custom_call" | custom-call | tf_op jit(solution)/shard_map/pallas_call | solution.py:413
  31.2 0.7 %shard_map.105 = (bf16[4,64,128]{2,1,0:T(8,128)(2,1)}, bf16[8,512]{1,0:T(8,128)(2,1)}) custom-call(bf16[4,64,128]{2,1,0:T(8,128)(2,1)S(1)} %get-tuple-element.4.cache, bf16[8,512]{1,0:T(8,128)(2,1)S(1)} %get-tuple-element.5.read), custom_call_target="tpu_custom_call" | custom-call | tf_op jit(solution)/shard_map/pallas_call | solution.py:463

commit v3 on v2

v3 whole, which is shorter than its diff:
```python
import functools

import jax
import jax.numpy as jnp
from jax import lax
from jax.experimental import pallas as pl
from jax.experimental.pallas import tpu as pltpu
from jax.sharding import PartitionSpec as P

EPSILON = 1e-06
RANGE = 166.0
TINY = 1e-30
MESH = pl.DeviceIdType.MESH
F32 = jnp.float32
BF16 = jnp.bfloat16


def partner(mine, step, count):
    total, bit = mine, 1
    while bit < count:
        if step // bit % 2:
            total = total + bit * (1 - 2 * lax.rem(mine // bit, 2))
        bit *= 2
    return total


def pieces(x, count):
    out = []
    for _ in range(count):
        piece = x.astype(BF16)
        out.append(piece)
        x = x - piece.astype(F32)
    return out


def arrival_order(members):
    if members == 8:
        return (0, 7, 3, 4, 5, 2, 6, 1)
    return (0,) + tuple(range(members - 1, 0, -1))


def encode(x):
    most = jnp.maximum(jnp.max(jnp.abs(x), axis=0, keepdims=True), TINY)
    level = jnp.exp(RANGE * (jnp.abs(x) * (1.0 / most) - 0.5))
    return jnp.where(x < 0.0, -level, level).astype(BF16), most


def decode(code, most):
    level = code.astype(F32)
    size = (jnp.log(jnp.abs(level)) * (1.0 / RANGE) + 0.5) * most
    return jnp.where(level < 0.0, -size, size)


def kernel(
    sizes,
    prompt, keep, token, w_query, w_forget, w_value, w_outgate, floor, gain,
    cache_out, read_out,
    stage, blocks, keeps, tokens, wq, wf, wv, wo, floors, gains,
    weighted, values, logs, decays, mine_early, early, states, codes, scales, got_codes, got_scales, reads, sums,
    local_sem, stage_sem, other_sem, direct_send, direct_recv, keep_send, keep_recv, fwd_send, fwd_recv,
    token_send, token_recv, early_send, early_recv, scale_send, scale_recv, state_send, state_recv, read_send, read_recv, far_sem,
):
    n, t, s_count, members, cubes, heads, head, rows = sizes
    group = cubes
    me, core = lax.axis_index("sp"), lax.axis_index("tp")
    cube, place = me // members, lax.rem(me, members)
    model = prompt.shape[2]
    part = model // t
    positions = prompt.shape[1]
    width = heads * head
    order = arrival_order(members)
    pairs = members // 2
    batches = 2 if heads % 2 == 0 else 1
    batch = heads // batches

    def prompt_of(p):
        if members % 4:
            return p
        low = lax.rem(p, 4)
        return p - low + lax.rem(low, 2) * 2 + low // 2

    def columns(c):
        return pl.ds(pl.multiple_of(c * part, part), part)

    peers = [partner(place, r, members) for r in order]
    prompts = [prompt_of(p) for p in peers]
    mine = prompts[0]

    def staging(k, c, sem):
        return pltpu.make_async_copy(prompt.at[prompts[k], :, columns(c)], stage.at[k, :, columns(c)], sem)

    staged = [staging(k, core, stage_sem.at[k]) for k in range(members)]
    others = [lax.rem(core + o, t) for o in range(1, t)]
    local = [
        pltpu.make_async_copy(keep, keeps.at[0], local_sem.at[0]),
        pltpu.make_async_copy(token, tokens.at[core], local_sem.at[1]),
        pltpu.make_async_copy(floor, floors, local_sem.at[2]),
        pltpu.make_async_copy(gain, gains, local_sem.at[3]),
        pltpu.make_async_copy(prompt.at[mine], blocks.at[0], local_sem.at[4]),
        pltpu.make_async_copy(w_forget, wf, local_sem.at[5]),
        pltpu.make_async_copy(w_value, wv, local_sem.at[6]),
        pltpu.make_async_copy(w_query, wq, local_sem.at[7]),
        pltpu.make_async_copy(w_outgate, wo, local_sem.at[8]),
    ]

    staged[1].start()
    local[0].start()
    local[1].start()
    barrier = pltpu.get_barrier_semaphore()
    for k in range(1, members):
        pl.semaphore_signal(barrier, inc=1, device_id=(cube * members + peers[k], core), device_id_type=MESH)
    for o in range(1, cubes):
        pl.semaphore_signal(barrier, inc=1, device_id=(lax.rem(me + o * members, n), core), device_id_type=MESH)
    for o in range(1, t):
        pl.semaphore_signal(barrier, inc=1, device_id=(me, lax.rem(core + o, t)), device_id_type=MESH)
    for k in range(2, members):
        staged[k].start()
    staged[0].start()

    def direct(k):
        return pltpu.make_async_remote_copy(
            src_ref=stage.at[k, :, columns(core)],
            dst_ref=blocks.at[k, :, columns(core)],
            send_sem=direct_send, recv_sem=direct_recv.at[k - 1],
            device_id=(cube * members + peers[k], core), device_id_type=MESH,
        )

    def keep_copy(k):
        return pltpu.make_async_remote_copy(
            src_ref=keeps.at[0], dst_ref=keeps.at[k],
            send_sem=keep_send, recv_sem=keep_recv,
            device_id=(cube * members + peers[k], core), device_id_type=MESH,
        )

    def forward(k, o, c):
        piece = blocks.at[k, :, columns(c)]
        return pltpu.make_async_remote_copy(
            src_ref=piece, dst_ref=piece,
            send_sem=fwd_send.at[o - 1], recv_sem=fwd_recv.at[k - 1, o - 1],
            device_id=(me, lax.rem(core + o, t)), device_id_type=MESH,
        )

    def token_copy(o, c):
        return pltpu.make_async_remote_copy(
            src_ref=tokens.at[c], dst_ref=tokens.at[c],
            send_sem=token_send.at[o - 1], recv_sem=token_recv.at[o - 1],
            device_id=(me, lax.rem(core + o, t)), device_id_type=MESH,
        )

    def early_copy(o, k):
        return pltpu.make_async_remote_copy(
            src_ref=mine_early.at[k], dst_ref=early.at[me],
            send_sem=early_send, recv_sem=early_recv,
            device_id=(lax.rem(cube + o, cubes) * members + peers[k], core), device_id_type=MESH,
        )

    def keeper(g):
        return mine * group + g

    def scale_copy(g):
        return pltpu.make_async_remote_copy(
            src_ref=scales.at[g], dst_ref=got_scales.at[cube],
            send_sem=scale_send.at[g], recv_sem=scale_recv.at[cube],
            device_id=(keeper(g), core), device_id_type=MESH,
        )

    def state_copy(g, b):
        return pltpu.make_async_remote_copy(
            src_ref=codes.at[pl.ds(b * batch, batch), pl.ds(g * rows, rows), :],
            dst_ref=got_codes.at[cube, pl.ds(b * batch, batch)],
            send_sem=state_send.at[g], recv_sem=state_recv.at[cube],
            device_id=(keeper(g), core), device_id_type=MESH,
        )

    def read_copy(o, sender):
        return pltpu.make_async_remote_copy(
            src_ref=reads.at[sender], dst_ref=reads.at[sender],
            send_sem=read_send, recv_sem=read_recv,
            device_id=(lax.rem(me + o, n), core), device_id_type=MESH,
        )

    def many(ref, send, recv):
        return pltpu.make_async_remote_copy(
            src_ref=ref, dst_ref=ref, send_sem=send, recv_sem=recv,
            device_id=(lax.rem(me + 1, n), core), device_id_type=MESH,
        )

    all_keeps = many(keeps.at[pl.ds(1, members - 1)], keep_send, keep_recv)
    all_direct = many(blocks.at[pl.ds(1, members - 1), :, columns(core)], direct_send, direct_recv.at[0])
    all_early = many(early.at[pl.ds(0, n - members)], early_send, early_recv)
    all_reads = many(reads.at[pl.ds(0, n - 1)], read_send, read_recv)

    local[0].wait()
    local[1].wait()
    with jax.named_scope("barrier"):
        pl.semaphore_wait(barrier, members - 1 + cubes - 1 + t - 1)
    for k in range(1, members):
        pl.semaphore_signal(far_sem, inc=1, device_id=(cube * members + peers[k], core), device_id_type=MESH)
        keep_copy(k).start()
    for k in range(1, members):
        staged[k].wait()
        direct(k).start()
    for o in range(1, t):
        token_copy(o, core).start()
    for i, c in enumerate(others):
        for k in range(members):
            staging(k, c, other_sem.at[i]).start()
    for i in (2, 5, 6, 7, 8, 4, 3):
        local[i].start()

    with jax.named_scope("wlocal"):
        staged[0].wait()
        for i, c in enumerate(others):
            half = stage.at[:, :, columns(c)]
            pltpu.make_async_copy(half, half, other_sem.at[i]).wait()
        local[2].wait()
        local[5].wait()
    floor_row = floors[...]
    p0 = lax.broadcasted_iota(jnp.int32, (positions, positions), 0)
    p1 = lax.broadcasted_iota(jnp.int32, (positions, positions), 1)

    def column(row):
        return jnp.sum(jnp.where(p0 == p1, jnp.broadcast_to(row, (positions, positions)), 0.0), axis=1, keepdims=True)

    def losses(x, lanes):
        pre = jnp.dot(x, wf[:, lanes], preferred_element_type=F32)
        return floor_row[:, lanes] * (1.0 / (1.0 + jnp.exp(pre)))

    every = slice(0, width)
    with jax.named_scope("early"):
        half = members // 2
        for k in range(0, members, half):
            x = stage[k : k + half].reshape(half * positions, model)
            scale = jnp.concatenate([column(keeps[0, pl.ds(prompts[k + i], 1), :]) for i in range(half)], axis=0)
            log_forget = jnp.log(scale * (1.0 - losses(x, every))).reshape(half, positions, width)
            mine_early[k : k + half] = jnp.sum(log_forget, axis=1, keepdims=True)
        pl.semaphore_wait(far_sem, members - 1)
        for o in range(1, cubes):
            for k in range(members):
                early_copy(o, k).start()
        early[pl.ds(cube * members, members)] = jnp.zeros((members, 1, width), F32)

    with jax.named_scope("wlocal2"):
        for i in (6, 7, 8, 4, 3):
            local[i].wait()
        for o in range(1, t):
            token_copy(o, lax.rem(core - o + t, t)).wait_recv()
    with jax.named_scope("token"):
        feature = jnp.concatenate([tokens[c] for c in range(t)], axis=1)
        query = jnp.dot(feature, wq[...], preferred_element_type=F32)
        new_forget = jnp.dot(feature, wf[...], preferred_element_type=F32)
        new_value = jnp.dot(feature, wv[...], preferred_element_type=F32).astype(BF16).astype(F32)
        new_gate = jnp.dot(feature, wo[...], preferred_element_type=F32)
        new_loss = floor_row * (1.0 / (1.0 + jnp.exp(new_forget)))
        read_weight = query * (1.0 - new_loss)
        sums[0] = query * new_loss
        sums[1] = new_value
        sums[2] = new_gate * (1.0 / (1.0 + jnp.exp(-new_gate)))
        seq = lax.broadcasted_iota(jnp.int32, read_weight.shape, 0)
        picked = jnp.where(seq == mine, read_weight, 0.0)
        sums[3] = jnp.broadcast_to(jnp.sum(picked, axis=0, keepdims=True), read_weight.shape)

    def block_rows(k, count):
        return blocks[k : k + count].reshape(count * positions, model)

    def value(k, count, lanes):
        out = jnp.dot(block_rows(k, count), wv[:, lanes], preferred_element_type=F32).astype(BF16)
        values[k : k + count, :, lanes] = out.reshape(count, positions, -1)

    def forget(k, count, lanes):
        size = count * positions
        loss = losses(block_rows(k, count), lanes)
        scale = jnp.concatenate([column(keeps[k + i, pl.ds(mine, 1), :]) for i in range(count)], axis=0)
        log_forget = jnp.log(scale * (1.0 - loss))
        gate = 1.0 - scale + scale * loss
        j0 = lax.broadcasted_iota(jnp.int32, (size, size), 0)
        j1 = lax.broadcasted_iota(jnp.int32, (size, size), 1)
        later = jnp.where((j1 > j0) & (j0 // positions == j1 // positions), 1.0, 0.0).astype(BF16)
        inside = sum(jnp.dot(later, piece, preferred_element_type=F32) for piece in pieces(log_forget, 2))
        for i in range(count):
            first = i * positions
            logs[peers[k + i], :, lanes] = inside[first : first + 1] + log_forget[first : first + 1]
        weighted[k : k + count, :, lanes] = (gate * jnp.exp(inside)).reshape(count, positions, -1)

    def arrive(k):
        with jax.named_scope("w_direct"):
            direct(k).wait_recv()
        for o in range(1, t):
            forward(k, o, core).start()

    def ready(k):
        with jax.named_scope("w_fwd"):
            for o in range(1, t):
                forward(k, o, lax.rem(core - o + t, t)).wait_recv()

    arrive(1)
    all_keeps.wait_recv()
    for j in range(pairs):
        if j < pairs - 1:
            arrive(2 * j + 2)
            arrive(2 * j + 3)
        if j > 0:
            ready(2 * j)
        ready(2 * j + 1)
        if j < pairs - 1:
            with jax.named_scope("forget"):
                forget(2 * j, 2, every)
            with jax.named_scope("value"):
                value(2 * j, 2, every)

    with jax.named_scope("w_early"):
        all_early.wait_recv()
    after = jnp.zeros((1, width), F32)
    for c in range(1, cubes):
        block = early[c * members]
        for p in range(1, members):
            block = block + early[c * members + p]
        after = after + jnp.where(c > cube, block, 0.0)

    with jax.named_scope("tail_forget"):
        forget(members - 2, 2, every)
        value(members - 2, 2, every)
        suffix = after
        for p in reversed(range(members)):
            decays[p] = jnp.exp(suffix)
            suffix = suffix + logs[p]
    for b in range(batches):
        with jax.named_scope("tail_states"):
            for h in range(b * batch, (b + 1) * batch):
                own = slice(h * head, (h + 1) * head)
                w = jnp.concatenate(
                    [weighted[k, :, own] * decays[peers[k], :, own] for k in range(members)], axis=0
                )
                v = values[:, :, own].reshape(members * positions, head)
                states[h] = sum(
                    lax.dot_general(piece, v, (((0,), (0,)), ((), ())), preferred_element_type=F32)
                    for piece in pieces(w, 2)
                )
        if b == batches - 1:
            with jax.named_scope("sendreads"):
                for h in range(heads):
                    own = slice(h * head, (h + 1) * head)
                    reads[me, :, own] = jnp.dot(
                        sums[3, :, own], states[h], preferred_element_type=F32, precision=lax.Precision.HIGHEST
                    )[0:1]
                for o in range(n - 1, 0, -1):
                    read_copy(o, me).start()
        with jax.named_scope("tail_codes"):
            for h in range(b * batch, (b + 1) * batch):
                own = slice(h * head, (h + 1) * head)
                for g in range(group):
                    span = slice(g * rows, (g + 1) * rows)
                    codes[h, span], scales[g, :, own] = encode(states[h, span])
            for g in range(group):

                @pl.when(keeper(g) != me)
                def _():
                    if b == batches - 1:
                        scale_copy(g).start()
                    state_copy(g, b).start()

                @pl.when(keeper(g) == me)
                def _():
                    span = slice(g * rows, (g + 1) * rows)
                    got_codes[cube, b * batch : (b + 1) * batch] = codes[b * batch : (b + 1) * batch, span]
                    if b == batches - 1:
                        got_scales[cube] = scales[g]

    source = prompt_of(me // group)
    for c in range(cubes):

        @pl.when(c * members + source != me)
        @jax.named_scope("w_states")
        def _():
            for piece, arrived in ((got_scales.at[c], scale_recv.at[c]), (got_codes.at[c], state_recv.at[c])):
                pltpu.make_async_remote_copy(
                    src_ref=piece, dst_ref=piece,
                    send_sem=read_send, recv_sem=arrived,
                    device_id=(c * members + source, core), device_id_type=MESH,
                ).wait_recv()

    for h in range(heads):
        own = slice(h * head, (h + 1) * head)
        cache_out[h] = sum(decode(got_codes[c, h], got_scales[c, :, own]) for c in range(cubes)).astype(BF16)

    with jax.named_scope("w_reads"):
        all_reads.wait_recv()
    for s in range(s_count):
        row = jnp.zeros((1, width), F32)
        for c in range(cubes):
            row = row + reads[c * members + prompt_of(s)]
        sums[4, s : s + 1, :] = row
    for h in range(heads):
        lanes = slice(h * head, (h + 1) * head)
        mixed = sums[4, :, lanes] + jnp.sum(sums[0, :, lanes], axis=1, keepdims=True) * sums[1, :, lanes]
        normed = mixed * lax.rsqrt(jnp.mean(mixed * mixed, axis=1, keepdims=True) + EPSILON)
        read_out[:, lanes] = (normed * gains[...] * sums[2, :, lanes]).astype(BF16)

    all_keeps.wait_send()
    all_direct.wait_send()
    for o in range(1, t):
        token_copy(o, core).wait_send()
        many(blocks.at[pl.ds(1, members - 1), :, columns(core)], fwd_send.at[o - 1], read_recv).wait_send()
    all_early.wait_send()
    for g in range(group):

        @pl.when(keeper(g) != me)
        def _():
            scale_copy(g).wait_send()
            many(codes.at[:, pl.ds(g * rows, rows), :], state_send.at[g], read_recv).wait_send()

    all_reads.wait_send()


def hand_over(cache, read, cache_out, read_out, sem):
    copies = [pltpu.make_async_copy(cache, cache_out, sem.at[0]), pltpu.make_async_copy(read, read_out, sem.at[1])]
    for copy in copies:
        copy.start()
    for copy in copies:
        copy.wait()


def per_device(prompt, keep_scale, new_token, w_query, w_forget, w_value, w_outgate, floor_gap, norm_gain):
    n, t = lax.axis_size("sp"), lax.axis_size("tp")
    s_count, positions, model = prompt.shape
    head = norm_gain.shape[0]
    width = w_forget.shape[1]
    heads = width // head
    members = s_count
    cubes = n // members
    group = cubes
    rows = head // group
    batches = 2 if heads % 2 == 0 else 1
    sizes = (n, t, s_count, members, cubes, heads, head, rows)
    dma = pltpu.SemaphoreType.DMA
    vmem = pl.BlockSpec(memory_space=pltpu.VMEM)
    hbm = pl.BlockSpec(memory_space=pltpu.HBM)
    cache, read = pl.pallas_call(
        functools.partial(kernel, sizes),
        out_shape=(
            pltpu.VMEM((heads, rows, head), BF16),
            pltpu.VMEM((s_count, width), BF16),
        ),
        in_specs=[hbm] * 9,
        out_specs=(vmem, vmem),
        scratch_shapes=[
            pltpu.VMEM((members, positions, model), BF16),
            pltpu.VMEM((members, positions, model), BF16),
            pltpu.VMEM((members,) + keep_scale.shape, F32),
            pltpu.VMEM((t,) + new_token.shape, BF16),
            pltpu.VMEM((model, width), BF16),
            pltpu.VMEM((model, width), BF16),
            pltpu.VMEM((model, width), BF16),
            pltpu.VMEM((model, width), BF16),
            pltpu.VMEM((1, width), F32),
            pltpu.VMEM((1, head), F32),
            pltpu.VMEM((members, positions, width), F32),
            pltpu.VMEM((members, positions, width), BF16),
            pltpu.VMEM((members, 1, width), F32),
            pltpu.VMEM((members, 1, width), F32),
            pltpu.VMEM((members, 1, width), F32),
            pltpu.VMEM((n, 1, width), F32),
            pltpu.VMEM((heads, head, head), F32),
            pltpu.VMEM((heads, head, head), BF16),
            pltpu.VMEM((group, 1, width), F32),
            pltpu.VMEM((cubes, heads, rows, head), BF16),
            pltpu.VMEM((cubes, 1, width), F32),
            pltpu.VMEM((n, 1, width), F32),
            pltpu.VMEM((5, s_count, width), F32),
            dma((9,)), dma((members,)), dma((t - 1,)),
            dma, dma((members - 1,)),
            dma, dma,
            dma((t - 1,)), dma((members - 1, t - 1)),
            dma((t - 1,)), dma((t - 1,)),
            dma, dma,
            dma((group,)), dma((cubes,)),
            dma((group,)), dma((cubes,)),
            dma, dma,
            pltpu.SemaphoreType.REGULAR,
        ],
        compiler_params=pltpu.CompilerParams(collective_id=0, has_side_effects=True, vmem_limit_bytes=32*1024*1024),
    )(
        *(
            pltpu.with_memory_space_constraint(x, pltpu.HBM)
            for x in (
                prompt, keep_scale, new_token, w_query, w_forget, w_value, w_outgate,
                floor_gap.reshape(1, width), norm_gain.reshape(1, head),
            )
        )
    )
    return pl.pallas_call(
        hand_over,
        out_shape=(
            jax.ShapeDtypeStruct((heads, rows, head), BF16),
            jax.ShapeDtypeStruct((s_count, width), BF16),
        ),
        in_specs=[vmem, vmem],
        out_specs=(pl.BlockSpec(memory_space=pltpu.HBM), pl.BlockSpec(memory_space=pltpu.HBM)),
        scratch_shapes=[dma((2,))],
        compiler_params=pltpu.CompilerParams(vmem_limit_bytes=1024*1024),
    )(cache, read)


def solution(mesh):
    return jax.shard_map(
        per_device,
        mesh=mesh,
        in_specs=(
            P(None, "sp", None),
            P(None, "sp"),
            P(None, "tp"),
            P(None, "tp"),
            P(None, "tp"),
            P(None, "tp"),
            P(None, "tp"),
            P("tp"),
            P(),
        ),
        out_specs=(P("tp", "sp", None), P(None, "tp")),
        check_vma=False,
    )
```

time: 32 us -> 30.3 us (0.947)
  Pallas kernels: 31.2 us -> 29.5 us
    pallas_call x1, Pallas kernels: 30.5 us -> 28.8 us  [per_device(): pl.pallas_call(functools.partial(kernel, sizes), out_shape=(pltpu.VMEM((h...]
where the time goes in v3:
time: 30.3 us; the launch traced here: 30.1 us
  Pallas kernels  29.5 us (97%)
  between operations  0.64 us (2%)
    pallas_call x1, Pallas kernels, per_device(): pl.pallas_call(functools.partial(kernel, sizes), out_shape=(pltpu.VMEM((h...  28.8 us
    pallas_call x1, Pallas kernels, per_device(): pl.pallas_call(hand_over, out_shape=(jax.ShapeDtypeStruct((heads, rows, h...  0.65 us

profile of v3, /device:TPU:0, one launch (start us, length us, event | category | flops | bytes accessed | tf_op | source)
XLA Modules:
  0.0 30.1 jit_solution(17245788614697674991)
XLA Ops:
  0.6 28.8 %shard_map.104 = (bf16[4,64,128]{2,1,0:T(8,128)(2,1)S(1)}, bf16[8,512]{1,0:T(8,128)(2,1)S(1)}) custom-call(bf16[8,64,2048]{2,1,0:T(8,128)(2,1)} %prompt.1, f32[8,64]{1,0:T(8,128)} %keep.1, bf16[8,1024]{1,0:T(8,128)(2,1)} %token_.1, bf16[2048,512]{1,0:T(8,128)(2,1)} %w_query.1, bf16[2048,512]{1,0:T(8,128)(2,1)} %w_forget.1, bf16[2048,512]{1,0:T(8,128)(2,1)} %w_value.1, ...), custom_call_target="tpu_custom_call" | custom-call | tf_op jit(solution)/shard_map/pallas_call | solution.py:438
  29.5 0.7 %shard_map.105 = (bf16[4,64,128]{2,1,0:T(8,128)(2,1)}, bf16[8,512]{1,0:T(8,128)(2,1)}) custom-call(bf16[4,64,128]{2,1,0:T(8,128)(2,1)S(1)} %get-tuple-element.4.cache, bf16[8,512]{1,0:T(8,128)(2,1)S(1)} %get-tuple-element.5.read), custom_call_target="tpu_custom_call" | custom-call | tf_op jit(solution)/shard_map/pallas_call | solution.py:491

commit v4 on v3

--- a/solution.py
+++ b/solution.py
@@ -55,8 +55,8 @@
     sizes,
     prompt, keep, token, w_query, w_forget, w_value, w_outgate, floor, gain,
     cache_out, read_out,
-    stage, blocks, keeps, tokens, wq, wf, wv, wo, floors, gains,
-    weighted, values, logs, decays, mine_early, early, states, codes, scales, got_codes, got_scales, reads, sums,
+    stage, blocks, keeps, rows_in, tokens, wf, weights, floors, gains,
+    weighted, values, logs, decays, mine_early, early, states, codes, scales, got_codes, got_scales, reads, sums, query_down,
     local_sem, stage_sem, other_sem, direct_send, direct_recv, keep_send, keep_recv, fwd_send, fwd_recv,
     token_send, token_recv, early_send, early_recv, scale_send, scale_recv, state_send, state_recv, read_send, read_recv, far_sem,
 ):
@@ -70,8 +70,6 @@
     width = heads * head
     order = arrival_order(members)
     pairs = members // 2
-    batches = 2 if heads % 2 == 0 else 1
-    batch = heads // batches
 
     def prompt_of(p):
         if members % 4:
@@ -89,7 +87,7 @@
     def staging(k, c, sem):
         return pltpu.make_async_copy(prompt.at[prompts[k], :, columns(c)], stage.at[k, :, columns(c)], sem)
 
-    staged = [staging(k, core, stage_sem.at[k]) for k in range(members)]
+    staged = [staging(k, core, stage_sem.at[1 if k == 1 else 0]) for k in range(members)]
     others = [lax.rem(core + o, t) for o in range(1, t)]
     local = [
         pltpu.make_async_copy(keep, keeps.at[0], local_sem.at[0]),
@@ -98,9 +96,9 @@
         pltpu.make_async_copy(gain, gains, local_sem.at[3]),
         pltpu.make_async_copy(prompt.at[mine], blocks.at[0], local_sem.at[4]),
         pltpu.make_async_copy(w_forget, wf, local_sem.at[5]),
-        pltpu.make_async_copy(w_value, wv, local_sem.at[6]),
-        pltpu.make_async_copy(w_query, wq, local_sem.at[7]),
-        pltpu.make_async_copy(w_outgate, wo, local_sem.at[8]),
+        pltpu.make_async_copy(w_value, weights.at[0], local_sem.at[6]),
+        pltpu.make_async_copy(w_query, weights.at[1], local_sem.at[6]),
+        pltpu.make_async_copy(w_outgate, weights.at[2], local_sem.at[6]),
     ]
 
     staged[1].start()
@@ -121,22 +119,25 @@
         return pltpu.make_async_remote_copy(
             src_ref=stage.at[k, :, columns(core)],
             dst_ref=blocks.at[k, :, columns(core)],
-            send_sem=direct_send, recv_sem=direct_recv.at[k - 1],
+            send_sem=direct_send, recv_sem=direct_recv.at[k // 2],
             device_id=(cube * members + peers[k], core), device_id_type=MESH,
         )
 
     def keep_copy(k):
         return pltpu.make_async_remote_copy(
-            src_ref=keeps.at[0], dst_ref=keeps.at[k],
+            src_ref=keeps.at[0, pl.ds(prompts[k], 1)], dst_ref=rows_in.at[k - 1],
             send_sem=keep_send, recv_sem=keep_recv,
             device_id=(cube * members + peers[k], core), device_id_type=MESH,
         )
 
-    def forward(k, o, c):
-        piece = blocks.at[k, :, columns(c)]
+    def landed(j, c):
+        return blocks.at[pl.ds(max(2 * j, 1), 2 if j else 1), :, columns(c)]
+
+    def forward(j, o, c):
+        piece = landed(j, c)
         return pltpu.make_async_remote_copy(
             src_ref=piece, dst_ref=piece,
-            send_sem=fwd_send.at[o - 1], recv_sem=fwd_recv.at[k - 1, o - 1],
+            send_sem=fwd_send.at[o - 1], recv_sem=fwd_recv.at[j, o - 1],
             device_id=(me, lax.rem(core + o, t)), device_id_type=MESH,
         )
 
@@ -164,10 +165,10 @@
             device_id=(keeper(g), core), device_id_type=MESH,
         )
 
-    def state_copy(g, b):
-        return pltpu.make_async_remote_copy(
-            src_ref=codes.at[pl.ds(b * batch, batch), pl.ds(g * rows, rows), :],
-            dst_ref=got_codes.at[cube, pl.ds(b * batch, batch)],
+    def state_copy(g):
+        return pltpu.make_async_remote_copy(
+            src_ref=codes.at[:, pl.ds(g * rows, rows), :],
+            dst_ref=got_codes.at[cube],
             send_sem=state_send.at[g], recv_sem=state_recv.at[cube],
             device_id=(keeper(g), core), device_id_type=MESH,
         )
@@ -185,21 +186,26 @@
             device_id=(lax.rem(me + 1, n), core), device_id_type=MESH,
         )
 
-    all_keeps = many(keeps.at[pl.ds(1, members - 1)], keep_send, keep_recv)
+    all_keeps = many(rows_in, keep_send, keep_recv)
     all_direct = many(blocks.at[pl.ds(1, members - 1), :, columns(core)], direct_send, direct_recv.at[0])
     all_early = many(early.at[pl.ds(0, n - members)], early_send, early_recv)
     all_reads = many(reads.at[pl.ds(0, n - 1)], read_send, read_recv)
 
-    local[0].wait()
-    local[1].wait()
     with jax.named_scope("barrier"):
         pl.semaphore_wait(barrier, members - 1 + cubes - 1 + t - 1)
+    staged[1].wait()
+    direct(1).start()
+    rest = stage.at[pl.ds(1, members - 1), :, columns(core)]
+    pltpu.make_async_copy(rest, rest, stage_sem.at[0]).wait()
+    for k in range(2, members):
+        direct(k).start()
+        if k == members // 2 - 1:
+            local[0].wait()
+            for i in range(1, members):
+                keep_copy(i).start()
     for k in range(1, members):
         pl.semaphore_signal(far_sem, inc=1, device_id=(cube * members + peers[k], core), device_id_type=MESH)
-        keep_copy(k).start()
-    for k in range(1, members):
-        staged[k].wait()
-        direct(k).start()
+    local[1].wait()
     for o in range(1, t):
         token_copy(o, core).start()
     for i, c in enumerate(others):
@@ -209,7 +215,6 @@
         local[i].start()
 
     with jax.named_scope("wlocal"):
-        staged[0].wait()
         for i, c in enumerate(others):
             half = stage.at[:, :, columns(c)]
             pltpu.make_async_copy(half, half, other_sem.at[i]).wait()
@@ -241,16 +246,17 @@
         early[pl.ds(cube * members, members)] = jnp.zeros((members, 1, width), F32)
 
     with jax.named_scope("wlocal2"):
-        for i in (6, 7, 8, 4, 3):
-            local[i].wait()
+        pltpu.make_async_copy(weights, weights, local_sem.at[6]).wait()
+        local[4].wait()
+        local[3].wait()
         for o in range(1, t):
             token_copy(o, lax.rem(core - o + t, t)).wait_recv()
     with jax.named_scope("token"):
         feature = jnp.concatenate([tokens[c] for c in range(t)], axis=1)
-        query = jnp.dot(feature, wq[...], preferred_element_type=F32)
+        query = jnp.dot(feature, weights[1], preferred_element_type=F32)
         new_forget = jnp.dot(feature, wf[...], preferred_element_type=F32)
-        new_value = jnp.dot(feature, wv[...], preferred_element_type=F32).astype(BF16).astype(F32)
-        new_gate = jnp.dot(feature, wo[...], preferred_element_type=F32)
+        new_value = jnp.dot(feature, weights[0], preferred_element_type=F32).astype(BF16).astype(F32)
+        new_gate = jnp.dot(feature, weights[2], preferred_element_type=F32)
         new_loss = floor_row * (1.0 / (1.0 + jnp.exp(new_forget)))
         read_weight = query * (1.0 - new_loss)
         sums[0] = query * new_loss
@@ -258,19 +264,25 @@
         sums[2] = new_gate * (1.0 / (1.0 + jnp.exp(-new_gate)))
         seq = lax.broadcasted_iota(jnp.int32, read_weight.shape, 0)
         picked = jnp.where(seq == mine, read_weight, 0.0)
-        sums[3] = jnp.broadcast_to(jnp.sum(picked, axis=0, keepdims=True), read_weight.shape)
+        weight = jnp.sum(picked, axis=0, keepdims=True)
+        h0 = lax.broadcasted_iota(jnp.int32, (head, head), 0)
+        h1 = lax.broadcasted_iota(jnp.int32, (head, head), 1)
+        for h in range(heads):
+            row = jnp.broadcast_to(weight[:, h * head : (h + 1) * head], (head, head))
+            down = jnp.sum(jnp.where(h0 == h1, row, 0.0), axis=1, keepdims=True)
+            query_down[h] = jnp.broadcast_to(down, (head, head))
 
     def block_rows(k, count):
         return blocks[k : k + count].reshape(count * positions, model)
 
     def value(k, count, lanes):
-        out = jnp.dot(block_rows(k, count), wv[:, lanes], preferred_element_type=F32).astype(BF16)
+        out = jnp.dot(block_rows(k, count), weights[0, :, lanes], preferred_element_type=F32).astype(BF16)
         values[k : k + count, :, lanes] = out.reshape(count, positions, -1)
 
     def forget(k, count, lanes):
         size = count * positions
         loss = losses(block_rows(k, count), lanes)
-        scale = jnp.concatenate([column(keeps[k + i, pl.ds(mine, 1), :]) for i in range(count)], axis=0)
+        scale = jnp.concatenate([column(rows_in[k + i - 1] if k + i else keeps[0, pl.ds(mine, 1), :]) for i in range(count)], axis=0)
         log_forget = jnp.log(scale * (1.0 - loss))
         gate = 1.0 - scale + scale * loss
         j0 = lax.broadcasted_iota(jnp.int32, (size, size), 0)
@@ -282,30 +294,23 @@
             logs[peers[k + i], :, lanes] = inside[first : first + 1] + log_forget[first : first + 1]
         weighted[k : k + count, :, lanes] = (gate * jnp.exp(inside)).reshape(count, positions, -1)
 
-    def arrive(k):
+    def arrive(j):
         with jax.named_scope("w_direct"):
-            direct(k).wait_recv()
+            many(landed(j, core), direct_send, direct_recv.at[j]).wait_recv()
         for o in range(1, t):
-            forward(k, o, core).start()
-
-    def ready(k):
-        with jax.named_scope("w_fwd"):
-            for o in range(1, t):
-                forward(k, o, lax.rem(core - o + t, t)).wait_recv()
-
-    arrive(1)
+            forward(j, o, core).start()
+
+    arrive(0)
     all_keeps.wait_recv()
     for j in range(pairs):
         if j < pairs - 1:
-            arrive(2 * j + 2)
-            arrive(2 * j + 3)
-        if j > 0:
-            ready(2 * j)
-        ready(2 * j + 1)
+            arrive(j + 1)
+        with jax.named_scope("w_fwd"):
+            for o in range(1, t):
+                forward(j, o, lax.rem(core - o + t, t)).wait_recv()
         if j < pairs - 1:
-            with jax.named_scope("forget"):
+            with jax.named_scope("pair"):
                 forget(2 * j, 2, every)
-            with jax.named_scope("value"):
                 value(2 * j, 2, every)
 
     with jax.named_scope("w_early"):
@@ -324,47 +329,37 @@
         for p in reversed(range(members)):
             decays[p] = jnp.exp(suffix)
             suffix = suffix + logs[p]
-    for b in range(batches):
-        with jax.named_scope("tail_states"):
-            for h in range(b * batch, (b + 1) * batch):
-                own = slice(h * head, (h + 1) * head)
-                w = jnp.concatenate(
-                    [weighted[k, :, own] * decays[peers[k], :, own] for k in range(members)], axis=0
-                )
-                v = values[:, :, own].reshape(members * positions, head)
-                states[h] = sum(
-                    lax.dot_general(piece, v, (((0,), (0,)), ((), ())), preferred_element_type=F32)
-                    for piece in pieces(w, 2)
-                )
-        if b == batches - 1:
-            with jax.named_scope("sendreads"):
-                for h in range(heads):
-                    own = slice(h * head, (h + 1) * head)
-                    reads[me, :, own] = jnp.dot(
-                        sums[3, :, own], states[h], preferred_element_type=F32, precision=lax.Precision.HIGHEST
-                    )[0:1]
-                for o in range(n - 1, 0, -1):
-                    read_copy(o, me).start()
-        with jax.named_scope("tail_codes"):
-            for h in range(b * batch, (b + 1) * batch):
-                own = slice(h * head, (h + 1) * head)
-                for g in range(group):
-                    span = slice(g * rows, (g + 1) * rows)
-                    codes[h, span], scales[g, :, own] = encode(states[h, span])
+    with jax.named_scope("tail_states"):
+        for h in range(heads):
+            own = slice(h * head, (h + 1) * head)
+            w = jnp.concatenate([weighted[k, :, own] * decays[peers[k], :, own] for k in range(members)], axis=0)
+            v = values[:, :, own].reshape(members * positions, head)
+            state = sum(
+                lax.dot_general(piece, v, (((0,), (0,)), ((), ())), preferred_element_type=F32)
+                for piece in pieces(w, 2)
+            )
+            states[h] = state
+            reads[me, :, own] = jnp.sum(query_down[h] * state, axis=0, keepdims=True)
+    with jax.named_scope("sendreads"):
+        for o in range(n - 1, 0, -1):
+            read_copy(o, me).start()
+    with jax.named_scope("tail_codes"):
+        for h in range(heads):
+            own = slice(h * head, (h + 1) * head)
             for g in range(group):
-
-                @pl.when(keeper(g) != me)
-                def _():
-                    if b == batches - 1:
-                        scale_copy(g).start()
-                    state_copy(g, b).start()
-
-                @pl.when(keeper(g) == me)
-                def _():
-                    span = slice(g * rows, (g + 1) * rows)
-                    got_codes[cube, b * batch : (b + 1) * batch] = codes[b * batch : (b + 1) * batch, span]
-                    if b == batches - 1:
-                        got_scales[cube] = scales[g]
+                span = slice(g * rows, (g + 1) * rows)
+                codes[h, span], scales[g, :, own] = encode(states[h, span])
+        for g in range(group):
+
+            @pl.when(keeper(g) != me)
+            def _():
+                scale_copy(g).start()
+                state_copy(g).start()
+
+            @pl.when(keeper(g) == me)
+            def _():
+                got_codes[cube] = codes[:, g * rows : (g + 1) * rows]
+                got_scales[cube] = scales[g]
 
     source = prompt_of(me // group)
     for c in range(cubes):
@@ -389,10 +384,10 @@
         row = jnp.zeros((1, width), F32)
         for c in range(cubes):
             row = row + reads[c * members + prompt_of(s)]
-        sums[4, s : s + 1, :] = row
+        sums[3, s : s + 1, :] = row
     for h in range(heads):
         lanes = slice(h * head, (h + 1) * head)
-        mixed = sums[4, :, lanes] + jnp.sum(sums[0, :, lanes], axis=1, keepdims=True) * sums[1, :, lanes]
+        mixed = sums[3, :, lanes] + jnp.sum(sums[0, :, lanes], axis=1, keepdims=True) * sums[1, :, lanes]
         normed = mixed * lax.rsqrt(jnp.mean(mixed * mixed, axis=1, keepdims=True) + EPSILON)
         read_out[:, lanes] = (normed * gains[...] * sums[2, :, lanes]).astype(BF16)
 
@@ -407,7 +402,7 @@
         @pl.when(keeper(g) != me)
         def _():
             scale_copy(g).wait_send()
-            many(codes.at[:, pl.ds(g * rows, rows), :], state_send.at[g], read_recv).wait_send()
+            state_copy(g).wait_send()
 
     all_reads.wait_send()
 
@@ -430,7 +425,6 @@
     cubes = n // members
     group = cubes
     rows = head // group
-    batches = 2 if heads % 2 == 0 else 1
     sizes = (n, t, s_count, members, cubes, heads, head, rows)
     dma = pltpu.SemaphoreType.DMA
     vmem = pl.BlockSpec(memory_space=pltpu.VMEM)
@@ -446,12 +440,11 @@
         scratch_shapes=[
             pltpu.VMEM((members, positions, model), BF16),
             pltpu.VMEM((members, positions, model), BF16),
-            pltpu.VMEM((members,) + keep_scale.shape, F32),
+            pltpu.VMEM((1,) + keep_scale.shape, F32),
+            pltpu.VMEM((members - 1, 1, positions), F32),
             pltpu.VMEM((t,) + new_token.shape, BF16),
             pltpu.VMEM((model, width), BF16),
-            pltpu.VMEM((model, width), BF16),
-            pltpu.VMEM((model, width), BF16),
-            pltpu.VMEM((model, width), BF16),
+            pltpu.VMEM((3, model, width), BF16),
             pltpu.VMEM((1, width), F32),
             pltpu.VMEM((1, head), F32),
             pltpu.VMEM((members, positions, width), F32),
@@ -466,11 +459,12 @@
             pltpu.VMEM((cubes, heads, rows, head), BF16),
             pltpu.VMEM((cubes, 1, width), F32),
             pltpu.VMEM((n, 1, width), F32),
-            pltpu.VMEM((5, s_count, width), F32),
-            dma((9,)), dma((members,)), dma((t - 1,)),
-            dma, dma((members - 1,)),
+            pltpu.VMEM((4, s_count, width), F32),
+            pltpu.VMEM((heads, head, head), F32),
+            dma((7,)), dma((2,)), dma((t - 1,)),
+            dma, dma((members // 2,)),
             dma, dma,
-            dma((t - 1,)), dma((members - 1, t - 1)),
+            dma((t - 1,)), dma((members // 2, t - 1)),
             dma((t - 1,)), dma((t - 1,)),
             dma, dma,
             dma((group,)), dma((cubes,)),

time: 30.3 us -> 28.7 us (0.947)
  Pallas kernels: 29.5 us -> 27.9 us
    pallas_call x1, Pallas kernels: 28.8 us -> 27.2 us  [per_device(): pl.pallas_call(functools.partial(kernel, sizes), out_shape=(pltpu.VMEM((h...]
where the time goes in v4:
time: 28.7 us; the launch traced here: 28.5 us
  Pallas kernels  27.9 us (97%)
  between operations  0.64 us (2%)
    pallas_call x1, Pallas kernels, per_device(): pl.pallas_call(functools.partial(kernel, sizes), out_shape=(pltpu.VMEM((h...  27.2 us
    pallas_call x1, Pallas kernels, per_device(): pl.pallas_call(hand_over, out_shape=(jax.ShapeDtypeStruct((heads, rows, h...  0.65 us

profile of v4, /device:TPU:0, one launch (start us, length us, event | category | flops | bytes accessed | tf_op | source)
XLA Modules:
  0.0 28.5 jit_solution(14754508105078461428)
XLA Ops:
  0.6 27.2 %shard_map.104 = (bf16[4,64,128]{2,1,0:T(8,128)(2,1)S(1)}, bf16[8,512]{1,0:T(8,128)(2,1)S(1)}) custom-call(bf16[8,64,2048]{2,1,0:T(8,128)(2,1)} %prompt.1, f32[8,64]{1,0:T(8,128)} %keep.1, bf16[8,1024]{1,0:T(8,128)(2,1)} %token_.1, bf16[2048,512]{1,0:T(8,128)(2,1)} %w_query.1, bf16[2048,512]{1,0:T(8,128)(2,1)} %w_forget.1, bf16[2048,512]{1,0:T(8,128)(2,1)} %w_value.1, ...), custom_call_target="tpu_custom_call" | custom-call | tf_op jit(solution)/shard_map/pallas_call | solution.py:432
  27.9 0.7 %shard_map.105 = (bf16[4,64,128]{2,1,0:T(8,128)(2,1)}, bf16[8,512]{1,0:T(8,128)(2,1)}) custom-call(bf16[4,64,128]{2,1,0:T(8,128)(2,1)S(1)} %get-tuple-element.4.cache, bf16[8,512]{1,0:T(8,128)(2,1)S(1)} %get-tuple-element.5.read), custom_call_target="tpu_custom_call" | custom-call | tf_op jit(solution)/shard_map/pallas_call | solution.py:485

commit v5 on v4

v5 whole, which is shorter than its diff:
```python
import functools

import jax
import jax.numpy as jnp
from jax import lax
from jax.experimental import pallas as pl
from jax.experimental.pallas import tpu as pltpu
from jax.sharding import PartitionSpec as P

EPSILON = 1e-06
RANGE = 166.0
TINY = 1e-30
MESH = pl.DeviceIdType.MESH
F32 = jnp.float32
BF16 = jnp.bfloat16


def partner(mine, step, count):
    total, bit = mine, 1
    while bit < count:
        if step // bit % 2:
            total = total + bit * (1 - 2 * lax.rem(mine // bit, 2))
        bit *= 2
    return total


def pieces(x, count):
    out = []
    for _ in range(count):
        piece = x.astype(BF16)
        out.append(piece)
        x = x - piece.astype(F32)
    return out


def arrival_order(members):
    if members == 8:
        return (0, 7, 4, 2, 3, 5, 6, 1)
    return (0,) + tuple(range(members - 1, 0, -1))


def encode(x, most):
    level = jnp.exp(RANGE * (jnp.abs(x) * (1.0 / most) - 0.5))
    return jnp.where(x < 0.0, -level, level).astype(BF16)


def size_of(code):
    return jnp.log(jnp.abs(code.astype(F32))) * (1.0 / RANGE) + 0.5


def decode(code, most):
    size = size_of(code) * most
    return jnp.where(code.astype(F32) < 0.0, -size, size)


def column_most(x):
    return jnp.maximum(jnp.max(jnp.abs(x), axis=0, keepdims=True), TINY)


def kernel(
    sizes,
    prompt, keep, token, w_query, w_forget, w_value, w_outgate, floor, gain,
    cache_out, read_out,
    stage, raw, keeps, rows_in, tokens, wf, wv, weights, floors, gains,
    payload, landed, weighted, values, decays, mine_early, early, cross,
    states, codes, scales, got_codes, got_scales, reads, spare, sums, query_down,
    local_sem, stage_sem, other_sem, raw_send, raw_recv, keep_send, keep_recv, fwd_send, fwd_recv,
    pay_send, pay_recv, cross_send, cross_recv,
    token_send, token_recv, early_send, early_recv, scale_send, scale_recv, state_send, state_recv, read_send, read_recv,
    far_sem,
):
    n, t, s_count, members, cubes, heads, head, rows = sizes
    group = cubes
    me, core = lax.axis_index("sp"), lax.axis_index("tp")
    cube, place = me // members, lax.rem(me, members)
    model = prompt.shape[2]
    part = model // t
    positions = prompt.shape[1]
    width = heads * head
    order = arrival_order(members)
    half = members // 2

    def prompt_of(p):
        if members % 4:
            return p
        low = lax.rem(p, 4)
        return p - low + lax.rem(low, 2) * 2 + low // 2

    def columns(c):
        return pl.ds(pl.multiple_of(c * part, part), part)

    peers = [partner(place, r, members) for r in order]
    prompts = [prompt_of(p) for p in peers]
    mine = prompts[0]
    others = [lax.rem(core + o, t) for o in range(1, t)]

    def mate(k):
        return cube * members + peers[k], core

    def staging(k, c, sem):
        return pltpu.make_async_copy(prompt.at[prompts[k], :, columns(c)], stage.at[k, :, columns(c)], sem)

    def sent(c):
        return stage.at[pl.ds(1, half - 1), :, columns(c)]

    def whole(k, sem):
        return pltpu.make_async_copy(prompt.at[prompts[k]], stage.at[k], sem)

    local = [
        pltpu.make_async_copy(keep, keeps.at[0], local_sem.at[0]),
        pltpu.make_async_copy(token, tokens.at[core], local_sem.at[1]),
        pltpu.make_async_copy(floor, floors, local_sem.at[2]),
        pltpu.make_async_copy(gain, gains, local_sem.at[3]),
        pltpu.make_async_copy(w_forget, wf, local_sem.at[4]),
        pltpu.make_async_copy(w_value, wv, local_sem.at[5]),
        pltpu.make_async_copy(w_query, weights.at[0], local_sem.at[6]),
        pltpu.make_async_copy(w_outgate, weights.at[1], local_sem.at[6]),
    ]

    for k in range(1, half):
        staging(k, core, stage_sem.at[0]).start()
    barrier = pltpu.get_barrier_semaphore()
    for k in range(1, members):
        pl.semaphore_signal(barrier, inc=1, device_id=mate(k), device_id_type=MESH)
    for o in range(1, cubes):
        pl.semaphore_signal(barrier, inc=1, device_id=(lax.rem(me + o * members, n), core), device_id_type=MESH)
    for o in range(1, t):
        pl.semaphore_signal(barrier, inc=1, device_id=(me, lax.rem(core + o, t)), device_id_type=MESH)
    local[0].start()
    local[2].start()
    local[4].start()
    for k in range(half, half + 2):
        whole(k, stage_sem.at[1]).start()
    local[5].start()
    for k in range(half + 2, members):
        whole(k, stage_sem.at[2]).start()
    whole(0, stage_sem.at[2]).start()
    for i, c in enumerate(others):
        for k in range(1, half):
            staging(k, c, other_sem.at[i]).start()
    for i in (1, 3, 6, 7):
        local[i].start()

    def raw_copy(k):
        return pltpu.make_async_remote_copy(
            src_ref=stage.at[k, :, columns(core)], dst_ref=raw.at[k - 1, :, columns(core)],
            send_sem=raw_send, recv_sem=raw_recv, device_id=mate(k), device_id_type=MESH,
        )

    def keep_copy(k):
        return pltpu.make_async_remote_copy(
            src_ref=keeps.at[0, pl.ds(prompts[k], 1)], dst_ref=rows_in.at[k - 1],
            send_sem=keep_send, recv_sem=keep_recv, device_id=mate(k), device_id_type=MESH,
        )

    def forward(o, c):
        piece = raw.at[:, :, columns(c)]
        return pltpu.make_async_remote_copy(
            src_ref=piece, dst_ref=piece,
            send_sem=fwd_send.at[o - 1], recv_sem=fwd_recv.at[o - 1],
            device_id=(me, lax.rem(core + o, t)), device_id_type=MESH,
        )

    def pay_copy(k):
        return pltpu.make_async_remote_copy(
            src_ref=payload.at[k - half], dst_ref=landed.at[k - half],
            send_sem=pay_send, recv_sem=pay_recv.at[(k - half) // 2],
            device_id=mate(k), device_id_type=MESH,
        )

    def token_copy(o, c):
        return pltpu.make_async_remote_copy(
            src_ref=tokens.at[c], dst_ref=tokens.at[c],
            send_sem=token_send.at[o - 1], recv_sem=token_recv.at[o - 1],
            device_id=(me, lax.rem(core + o, t)), device_id_type=MESH,
        )

    def early_copy(k):
        return pltpu.make_async_remote_copy(
            src_ref=mine_early.at[k], dst_ref=early.at[place],
            send_sem=early_send, recv_sem=early_recv,
            device_id=mate(k), device_id_type=MESH,
        )

    def cross_copy(c, k):
        return pltpu.make_async_remote_copy(
            src_ref=mine_early.at[k, 0], dst_ref=cross.at[cube, place],
            send_sem=cross_send.at[c], recv_sem=cross_recv.at[cube],
            device_id=(c * members + peers[k], core), device_id_type=MESH,
        )

    def keeper(g):
        return mine * group + g

    def scale_copy(g):
        return pltpu.make_async_remote_copy(
            src_ref=scales.at[g], dst_ref=got_scales.at[cube],
            send_sem=scale_send.at[g], recv_sem=scale_recv.at[cube],
            device_id=(keeper(g), core), device_id_type=MESH,
        )

    def state_copy(g):
        return pltpu.make_async_remote_copy(
            src_ref=codes.at[:, pl.ds(g * rows, rows), :],
            dst_ref=got_codes.at[cube],
            send_sem=state_send.at[g], recv_sem=state_recv.at[cube],
            device_id=(keeper(g), core), device_id_type=MESH,
        )

    def read_copy(o):
        piece = reads.at[cube, pl.ds(mine, 1)]
        return pltpu.make_async_remote_copy(
            src_ref=piece, dst_ref=piece,
            send_sem=read_send, recv_sem=read_recv,
            device_id=(lax.rem(me + o, n), core), device_id_type=MESH,
        )

    def many(ref, send, recv):
        return pltpu.make_async_remote_copy(
            src_ref=ref, dst_ref=ref, send_sem=send, recv_sem=recv,
            device_id=(lax.rem(me + 1, n), core), device_id_type=MESH,
        )

    all_raw = many(raw.at[:, :, columns(core)], raw_send, raw_recv)
    all_keeps = many(rows_in, keep_send, keep_recv)
    all_pay = many(landed, pay_send, pay_recv.at[0])
    all_early = many(early.at[pl.ds(0, members - 1)], early_send, early_recv)
    all_reads = many(spare, read_send, read_recv)

    with jax.named_scope("barrier"):
        pl.semaphore_wait(barrier, members - 1 + cubes - 1 + t - 1)
    pltpu.make_async_copy(sent(core), sent(core), stage_sem.at[0]).wait()
    for k in range(1, half):
        raw_copy(k).start()
    local[0].wait()
    for k in range(1, half):
        keep_copy(k).start()
    for k in range(1, members):
        pl.semaphore_signal(far_sem, inc=1, device_id=mate(k), device_id_type=MESH)

    with jax.named_scope("wlocal"):
        local[2].wait()
        local[4].wait()
        both = stage.at[pl.ds(half, 2)]
        pltpu.make_async_copy(both, both, stage_sem.at[1]).wait()
    floor_row = floors[...]
    p0 = lax.broadcasted_iota(jnp.int32, (positions, positions), 0)
    p1 = lax.broadcasted_iota(jnp.int32, (positions, positions), 1)

    def column(row):
        return jnp.sum(jnp.where(p0 == p1, jnp.broadcast_to(row, (positions, positions)), 0.0), axis=1, keepdims=True)

    def value(x):
        return jnp.dot(x, wv[...], preferred_element_type=F32).astype(BF16)

    def forget(x, keep_rows):
        size = x.shape[0]
        pre = jnp.dot(x, wf[...], preferred_element_type=F32)
        loss = floor_row * (1.0 / (1.0 + jnp.exp(pre)))
        scale = jnp.concatenate([column(row) for row in keep_rows], axis=0)
        log_forget = jnp.log(scale * (1.0 - loss))
        gate = 1.0 - scale + scale * loss
        j0 = lax.broadcasted_iota(jnp.int32, (size, size), 0)
        j1 = lax.broadcasted_iota(jnp.int32, (size, size), 1)
        later = jnp.where((j1 > j0) & (j0 // positions == j1 // positions), 1.0, 0.0).astype(BF16)
        inside = sum(jnp.dot(later, piece, preferred_element_type=F32) for piece in pieces(log_forget, 2))
        totals = [
            inside[first : first + 1] + log_forget[first : first + 1] for first in range(0, size, positions)
        ]
        return gate * jnp.exp(inside), totals

    def kept(k):
        return keeps[0, pl.ds(prompts[k], 1), :]

    def prepare(k):
        x = stage[k : k + 2].reshape(2 * positions, model)
        key, totals = forget(x, [kept(k), kept(k + 1)])
        if k == half:
            local[5].wait()
        fresh = value(x)
        for i in range(2):
            span = slice(i * positions, (i + 1) * positions)
            most = column_most(key[span])
            payload[k + i - half, :, :width] = encode(key[span], most)
            payload[k + i - half, :, width:] = fresh[span]
            mine_early[k + i, 0] = totals[i]
            mine_early[k + i, 1] = most

    with jax.named_scope("prepare"):
        for k in range(half, members, 2):
            if k > half:
                rest = stage.at[pl.ds(half + 1, half - 1)]
                pltpu.make_async_copy(rest, rest, stage_sem.at[2]).wait()
            prepare(k)
            if k == half:
                pay_copy(k).start()
                pay_copy(k + 1).start()
    with jax.named_scope("own"):
        for i, c in enumerate(others):
            pltpu.make_async_copy(sent(c), sent(c), other_sem.at[i]).wait()
        x = stage[0:half].reshape(half * positions, model)
        key, totals = forget(x, [kept(k) for k in range(half)])
        weighted[0] = key[:positions]
        for k in range(half):
            mine_early[k, 0] = totals[k]
            mine_early[k, 1] = totals[k]
        early[place, 0] = totals[0]
        pl.semaphore_wait(far_sem, members - 1)
        for c in range(cubes - 1):

            @pl.when(c < cube)
            def _():
                for k in range(members):
                    cross_copy(c, k).start()

        for k in range(1, members):
            early_copy(k).start()
        values[0] = value(stage[0])

    with jax.named_scope("wlocal2"):
        local[1].wait()
        for o in range(1, t):
            token_copy(o, core).start()
        local[3].wait()
        pltpu.make_async_copy(weights, weights, local_sem.at[6]).wait()
        for o in range(1, t):
            token_copy(o, lax.rem(core - o + t, t)).wait_recv()
    with jax.named_scope("token"):
        feature = jnp.concatenate([tokens[c] for c in range(t)], axis=1)
        query = jnp.dot(feature, weights[0], preferred_element_type=F32)
        new_forget = jnp.dot(feature, wf[...], preferred_element_type=F32)
        new_value = jnp.dot(feature, wv[...], preferred_element_type=F32).astype(BF16).astype(F32)
        new_gate = jnp.dot(feature, weights[1], preferred_element_type=F32)
        new_loss = floor_row * (1.0 / (1.0 + jnp.exp(new_forget)))
        read_weight = query * (1.0 - new_loss)
        silu = new_gate * (1.0 / (1.0 + jnp.exp(-new_gate)))
        fresh = query * new_loss
        for h in range(heads):
            own = slice(h * head, (h + 1) * head)
            sums[0, :, own] = jnp.sum(fresh[:, own], axis=1, keepdims=True) * new_value[:, own]
            sums[1, :, own] = gains[...] * silu[:, own]
        seq = lax.broadcasted_iota(jnp.int32, read_weight.shape, 0)
        picked = jnp.where(seq == mine, read_weight, 0.0)
        weight = jnp.sum(picked, axis=0, keepdims=True)
        h0 = lax.broadcasted_iota(jnp.int32, (head, head), 0)
        h1 = lax.broadcasted_iota(jnp.int32, (head, head), 1)
        for h in range(heads):
            row = jnp.broadcast_to(weight[:, h * head : (h + 1) * head], (head, head))
            down = jnp.sum(jnp.where(h0 == h1, row, 0.0), axis=1, keepdims=True)
            query_down[h] = jnp.broadcast_to(down, (head, head))

    def add_up(first, last, start):
        found = []
        for h in range(heads):
            own = slice(h * head, (h + 1) * head)
            keys, fresh = [], []
            for k in range(first, last):
                decay = decays[peers[k], :, own]
                if k < half:
                    keys.append(weighted[k, :, own] * decay)
                    fresh.append(values[k, :, own])
                else:
                    keys.append(size_of(landed[k - half, :, own]) * (early[peers[k], 1, :, own] * decay))
                    fresh.append(landed[k - half, :, width + h * head : width + (h + 1) * head])
            keys, fresh = jnp.concatenate(keys, axis=0), jnp.concatenate(fresh, axis=0)
            state = sum(
                lax.dot_general(piece, fresh, (((0,), (0,)), ((), ())), preferred_element_type=F32)
                for piece in pieces(keys, 2)
            )
            state = state if start else states[h] + state
            states[h] = state
            found.append(jnp.sum(query_down[h] * state, axis=0, keepdims=True))
        return found

    def arrive(j):
        with jax.named_scope("w_pay"):
            many(landed.at[pl.ds(2 * j, 2)], pay_send, pay_recv.at[j]).wait_recv()

    for k in range(half + 2, members):
        pay_copy(k).start()
    with jax.named_scope("w_raw"):
        all_raw.wait_recv()
        for o in range(1, t):
            forward(o, core).start()
        all_keeps.wait_recv()
        for o in range(1, t):
            forward(o, lax.rem(core - o + t, t)).wait_recv()
    with jax.named_scope("raw"):
        x = raw[...].reshape((half - 1) * positions, model)
        key, _ = forget(x, [rows_in[k] for k in range(half - 1)])
        weighted[1:half] = key.reshape(half - 1, positions, width)
        values[1:half] = value(x).reshape(half - 1, positions, width)
    with jax.named_scope("w_early"):
        all_early.wait_recv()
        for c in range(1, cubes):

            @pl.when(c > cube)
            def _():
                many(cross.at[c], cross_send.at[0], cross_recv.at[c]).wait_recv()

            @pl.when(c <= cube)
            def _():
                cross[c] = jnp.zeros((members, 1, width), F32)

    with jax.named_scope("decays"):
        suffix = jnp.zeros((1, width), F32)
        for c in range(1, cubes):
            for p in range(members):
                suffix = suffix + cross[c, p]
        for p in reversed(range(members)):
            decays[p] = jnp.exp(suffix)
            suffix = suffix + early[p, 0]
    tail = half // 2 - 1
    for j in range(tail):
        arrive(j)
    with jax.named_scope("states"):
        add_up(0, members - 2, True)
    arrive(tail)
    with jax.named_scope("tail_states"):
        found = add_up(members - 2, members, False)
        reads[cube, pl.ds(mine, 1), :] = jnp.concatenate(found, axis=1)
    with jax.named_scope("sendreads"):
        for o in range(n - 1, 0, -1):
            read_copy(o).start()
    with jax.named_scope("tail_codes"):
        for h in range(heads):
            own = slice(h * head, (h + 1) * head)
            for g in range(group):
                span = slice(g * rows, (g + 1) * rows)
                most = column_most(states[h, span])
                codes[h, span], scales[g, :, own] = encode(states[h, span], most), most
        for g in range(group):

            @pl.when(keeper(g) != me)
            def _():
                scale_copy(g).start()
                state_copy(g).start()

            @pl.when(keeper(g) == me)
            def _():
                got_codes[cube] = codes[:, g * rows : (g + 1) * rows]
                got_scales[cube] = scales[g]

    source = prompt_of(me // group)
    for c in range(cubes):

        @pl.when(c * members + source != me)
        @jax.named_scope("w_states")
        def _():
            for piece, arrived in ((got_scales.at[c], scale_recv.at[c]), (got_codes.at[c], state_recv.at[c])):
                pltpu.make_async_remote_copy(
                    src_ref=piece, dst_ref=piece,
                    send_sem=read_send, recv_sem=arrived,
                    device_id=(c * members + source, core), device_id_type=MESH,
                ).wait_recv()

    for h in range(heads):
        own = slice(h * head, (h + 1) * head)
        cache_out[h] = sum(decode(got_codes[c, h], got_scales[c, :, own]) for c in range(cubes)).astype(BF16)

    with jax.named_scope("w_reads"):
        all_reads.wait_recv()
    mixed = sums[0]
    for c in range(cubes):
        mixed = mixed + reads[c]
    for h in range(heads):
        own = slice(h * head, (h + 1) * head)
        part_mixed = mixed[:, own]
        spread = lax.rsqrt(jnp.mean(part_mixed * part_mixed, axis=1, keepdims=True) + EPSILON)
        read_out[:, own] = (part_mixed * spread * sums[1, :, own]).astype(BF16)

    all_raw.wait_send()
    all_keeps.wait_send()
    all_pay.wait_send()
    for o in range(1, t):
        token_copy(o, core).wait_send()
        forward(o, core).wait_send()
    all_early.wait_send()
    for c in range(cubes - 1):

        @pl.when(c < cube)
        def _():
            many(cross.at[0], cross_send.at[c], early_recv).wait_send()

    for g in range(group):

        @pl.when(keeper(g) != me)
        def _():
            scale_copy(g).wait_send()
            state_copy(g).wait_send()

    all_reads.wait_send()


def hand_over(cache, read, cache_out, read_out, sem):
    copies = [pltpu.make_async_copy(cache, cache_out, sem.at[0]), pltpu.make_async_copy(read, read_out, sem.at[1])]
    for copy in copies:
        copy.start()
    for copy in copies:
        copy.wait()


def per_device(prompt, keep_scale, new_token, w_query, w_forget, w_value, w_outgate, floor_gap, norm_gain):
    n, t = lax.axis_size("sp"), lax.axis_size("tp")
    s_count, positions, model = prompt.shape
    head = norm_gain.shape[0]
    width = w_forget.shape[1]
    heads = width // head
    members = s_count
    cubes = n // members
    group = cubes
    rows = head // group
    sizes = (n, t, s_count, members, cubes, heads, head, rows)
    dma = pltpu.SemaphoreType.DMA
    vmem = pl.BlockSpec(memory_space=pltpu.VMEM)
    hbm = pl.BlockSpec(memory_space=pltpu.HBM)
    cache, read = pl.pallas_call(
        functools.partial(kernel, sizes),
        out_shape=(
            pltpu.VMEM((heads, rows, head), BF16),
            pltpu.VMEM((s_count, width), BF16),
        ),
        in_specs=[hbm] * 9,
        out_specs=(vmem, vmem),
        scratch_shapes=[
            pltpu.VMEM((members, positions, model), BF16),
            pltpu.VMEM((members // 2 - 1, positions, model), BF16),
            pltpu.VMEM((1,) + keep_scale.shape, F32),
            pltpu.VMEM((members // 2 - 1, 1, positions), F32),
            pltpu.VMEM((t,) + new_token.shape, BF16),
            pltpu.VMEM((model, width), BF16),
            pltpu.VMEM((model, width), BF16),
            pltpu.VMEM((2, model, width), BF16),
            pltpu.VMEM((1, width), F32),
            pltpu.VMEM((1, head), F32),
            pltpu.VMEM((members // 2, positions, 2 * width), BF16),
            pltpu.VMEM((members // 2, positions, 2 * width), BF16),
            pltpu.VMEM((members // 2, positions, width), F32),
            pltpu.VMEM((members // 2, positions, width), BF16),
            pltpu.VMEM((members, 1, width), F32),
            pltpu.VMEM((members, 2, 1, width), F32),
            pltpu.VMEM((members, 2, 1, width), F32),
            pltpu.VMEM((cubes, members, 1, width), F32),
            pltpu.VMEM((heads, head, head), F32),
            pltpu.VMEM((heads, head, head), BF16),
            pltpu.VMEM((group, 1, width), F32),
            pltpu.VMEM((cubes, heads, rows, head), BF16),
            pltpu.VMEM((cubes, 1, width), F32),
            pltpu.VMEM((cubes, s_count, width), F32),
            pltpu.VMEM((n - 1, 1, width), F32),
            pltpu.VMEM((2, s_count, width), F32),
            pltpu.VMEM((heads, head, head), F32),
            dma((7,)), dma((3,)), dma((t - 1,)),
            dma, dma, dma, dma,
            dma((t - 1,)), dma((t - 1,)),
            dma, dma((members // 4,)),
            dma((cubes - 1,)), dma((cubes,)),
            dma((t - 1,)), dma((t - 1,)),
            dma, dma,
            dma((group,)), dma((cubes,)),
            dma((group,)), dma((cubes,)),
            dma, dma,
            pltpu.SemaphoreType.REGULAR,
        ],
        compiler_params=pltpu.CompilerParams(collective_id=0, has_side_effects=True, vmem_limit_bytes=32*1024*1024),
    )(
        *(
            pltpu.with_memory_space_constraint(x, pltpu.HBM)
            for x in (
                prompt, keep_scale, new_token, w_query, w_forget, w_value, w_outgate,
                floor_gap.reshape(1, width), norm_gain.reshape(1, head),
            )
        )
    )
    return pl.pallas_call(
        hand_over,
        out_shape=(
            jax.ShapeDtypeStruct((heads, rows, head), BF16),
            jax.ShapeDtypeStruct((s_count, width), BF16),
        ),
        in_specs=[vmem, vmem],
        out_specs=(pl.BlockSpec(memory_space=pltpu.HBM), pl.BlockSpec(memory_space=pltpu.HBM)),
        scratch_shapes=[dma((2,))],
        compiler_params=pltpu.CompilerParams(vmem_limit_bytes=1024*1024),
    )(cache, read)


def solution(mesh):
    return jax.shard_map(
        per_device,
        mesh=mesh,
        in_specs=(
            P(None, "sp", None),
            P(None, "sp"),
            P(None, "tp"),
            P(None, "tp"),
            P(None, "tp"),
            P(None, "tp"),
            P(None, "tp"),
            P("tp"),
            P(),
        ),
        out_specs=(P("tp", "sp", None), P(None, "tp")),
        check_vma=False,
    )
```

time: 28.7 us -> 26.8 us (0.934)
  Pallas kernels: 27.9 us -> 25.8 us
    pallas_call x1, Pallas kernels: 27.2 us -> 25.2 us  [per_device(): pl.pallas_call(functools.partial(kernel, sizes), out_shape=(pltpu.VMEM((h...]
where the time goes in v5:
time: 26.8 us; the launch traced here: 26.5 us
  Pallas kernels  25.8 us (96%)
  between operations  0.64 us (2%)
    pallas_call x1, Pallas kernels, per_device(): pl.pallas_call(functools.partial(kernel, sizes), out_shape=(pltpu.VMEM((h...  25.2 us
    pallas_call x1, Pallas kernels, per_device(): pl.pallas_call(hand_over, out_shape=(jax.ShapeDtypeStruct((heads, rows, h...  0.65 us

profile of v5, /device:TPU:0, one launch (start us, length us, event | category | flops | bytes accessed | tf_op | source)
XLA Modules:
  0.0 26.5 jit_solution(8400246502311272496)
XLA Ops:
  0.6 25.2 %shard_map.104 = (bf16[4,64,128]{2,1,0:T(8,128)(2,1)S(1)}, bf16[8,512]{1,0:T(8,128)(2,1)S(1)}) custom-call(bf16[8,64,2048]{2,1,0:T(8,128)(2,1)} %prompt.1, f32[8,64]{1,0:T(8,128)} %keep.1, bf16[8,1024]{1,0:T(8,128)(2,1)} %token_.1, bf16[2048,512]{1,0:T(8,128)(2,1)} %w_query.1, bf16[2048,512]{1,0:T(8,128)(2,1)} %w_forget.1, bf16[2048,512]{1,0:T(8,128)(2,1)} %w_value.1, ...), custom_call_target="tpu_custom_call" | custom-call | tf_op jit(solution)/shard_map/pallas_call | solution.py:517
  25.8 0.7 %shard_map.105 = (bf16[4,64,128]{2,1,0:T(8,128)(2,1)}, bf16[8,512]{1,0:T(8,128)(2,1)}) custom-call(bf16[4,64,128]{2,1,0:T(8,128)(2,1)S(1)} %get-tuple-element.4.cache, bf16[8,512]{1,0:T(8,128)(2,1)S(1)} %get-tuple-element.5.read), custom_call_target="tpu_custom_call" | custom-call | tf_op jit(solution)/shard_map/pallas_call | solution.py:575

commit v6 on v5

--- a/solution.py
+++ b/solution.py
@@ -42,6 +42,15 @@
 def encode(x, most):
     level = jnp.exp(RANGE * (jnp.abs(x) * (1.0 / most) - 0.5))
     return jnp.where(x < 0.0, -level, level).astype(BF16)
+
+
+def encode_key(x, most):
+    return jnp.exp(RANGE * (jnp.sqrt(jnp.sqrt(jnp.maximum(x * (1.0 / most), TINY))) - 0.5)).astype(BF16)
+
+
+def key_of(code):
+    root = size_of(code)
+    return (root * root) * (root * root)
 
 
 def size_of(code):
@@ -281,7 +290,7 @@
         for i in range(2):
             span = slice(i * positions, (i + 1) * positions)
             most = column_most(key[span])
-            payload[k + i - half, :, :width] = encode(key[span], most)
+            payload[k + i - half, :, :width] = encode_key(key[span], most)
             payload[k + i - half, :, width:] = fresh[span]
             mine_early[k + i, 0] = totals[i]
             mine_early[k + i, 1] = most
@@ -360,7 +369,7 @@
                     keys.append(weighted[k, :, own] * decay)
                     fresh.append(values[k, :, own])
                 else:
-                    keys.append(size_of(landed[k - half, :, own]) * (early[peers[k], 1, :, own] * decay))
+                    keys.append(key_of(landed[k - half, :, own]) * (early[peers[k], 1, :, own] * decay))
                     fresh.append(landed[k - half, :, width + h * head : width + (h + 1) * head])
             keys, fresh = jnp.concatenate(keys, axis=0), jnp.concatenate(fresh, axis=0)
             state = sum(

time: 26.8 us -> 26.8 us (level)
  no operation moved by 1% of the time
where the time goes in v6:
time: 26.8 us; the launch traced here: 26.5 us
  Pallas kernels  25.8 us (96%)
  between operations  0.64 us (2%)
    pallas_call x1, Pallas kernels, per_device(): pl.pallas_call(functools.partial(kernel, sizes), out_shape=(pltpu.VMEM((h...  25.2 us
    pallas_call x1, Pallas kernels, per_device(): pl.pallas_call(hand_over, out_shape=(jax.ShapeDtypeStruct((heads, rows, h...  0.65 us

profile of v6, /device:TPU:0, one launch (start us, length us, event | category | flops | bytes accessed | tf_op | source)
XLA Modules:
  0.0 26.5 jit_solution(8763439482014382094)
XLA Ops:
  0.6 25.2 %shard_map.104 = (bf16[4,64,128]{2,1,0:T(8,128)(2,1)S(1)}, bf16[8,512]{1,0:T(8,128)(2,1)S(1)}) custom-call(bf16[8,64,2048]{2,1,0:T(8,128)(2,1)} %prompt.1, f32[8,64]{1,0:T(8,128)} %keep.1, bf16[8,1024]{1,0:T(8,128)(2,1)} %token_.1, bf16[2048,512]{1,0:T(8,128)(2,1)} %w_query.1, bf16[2048,512]{1,0:T(8,128)(2,1)} %w_forget.1, bf16[2048,512]{1,0:T(8,128)(2,1)} %w_value.1, ...), custom_call_target="tpu_custom_call" | custom-call | tf_op jit(solution)/shard_map/pallas_call | solution.py:526
  25.8 0.7 %shard_map.105 = (bf16[4,64,128]{2,1,0:T(8,128)(2,1)}, bf16[8,512]{1,0:T(8,128)(2,1)}) custom-call(bf16[4,64,128]{2,1,0:T(8,128)(2,1)S(1)} %get-tuple-element.4.cache, bf16[8,512]{1,0:T(8,128)(2,1)S(1)} %get-tuple-element.5.read), custom_call_target="tpu_custom_call" | custom-call | tf_op jit(solution)/shard_map/pallas_call | solution.py:584
